TPU v7x, 32 devices: a whole 2x2x4 slice. The times are simulated.
32 devices in a mesh: sp: 8 (over z, y), tp: 4 (over x, core).
Axes of the slice: x: 2, y: 2, z: 4, core: 2. Of those that a mesh axis runs over, the one named last changes fastest.
Arguments:
- tokens: bfloat16 [6144, 2048], P('sp', 'tp'), may hold values from -6 to 6
- norm_gain: float32 [2048], replicated, may hold values from 0.1 to 1.9
- w_query: bfloat16 [2048, 2048], P(None, 'tp'), may hold values from -4 to 4
- w_key: bfloat16 [2048, 2048], P(None, 'tp'), may hold values from -4 to 4
- w_value: bfloat16 [2048, 2048], P(None, 'tp'), may hold values from -0.125 to 0.125
- w_outer: bfloat16 [2048, 2048], P(None, 'tp'), may hold values from -0.125 to 0.125
- w_inner: bfloat16 [2048, 2048], P(None, 'tp'), may hold values from -0.125 to 0.125
- w_signal: bfloat16 [2048, 2048], P(None, 'tp'), may hold values from -0.125 to 0.125
- conv_taps: bfloat16 [3, 2048], P(None, 'tp'), may hold values from -3.5 to 3.5
- lambdas: float32 [8], P('tp'), may hold values from 0.3 to 0.8
- head_gain: float32 [256], replicated, may hold values from 0.1 to 1.9
- attend_proj: bfloat16 [2048, 2048], P('tp'), may hold values from -0.125 to 0.125
- convolve_proj: bfloat16 [2048, 2048], P('tp'), may hold values from -0.125 to 0.125
Outputs:
- mixed: bfloat16 [6144, 2048], P(('sp', 'tp'))
- row_lse: float32 [6144, 16], P('sp', 'tp')
All inputs are finite; a program needn't handle non-finite values.
Results may differ from a plain program's by a relative error of at most 0.015.
Values may be sent and summed in bfloat16 or wider, within the bound.
A program may use at most 128 MiB of HBM per device.

v0:
```python
import jax
import jax.numpy as jnp
from jax import lax
from jax.sharding import PartitionSpec as P

ROPE_BASE = 500000.0
NORM_EPS = 1e-05
HEAD_KEEP = 0.8
MASKED = -1e30


def partner(value, axis, stride):
    return lax.ppermute(value, axis, [(i, i ^ 1 << stride) for i in range(lax.axis_size(axis))])


def passed_along(value, axis, steps):
    count = lax.axis_size(axis)
    initial, last = (max(0, -steps), min(count, count - steps))
    return lax.ppermute(value, axis, [(source, source + steps) for source in range(initial, last)])


def rotate(values_in, positions):
    half_width = values_in.shape[-1] // 2
    inverse = ROPE_BASE ** (-jnp.arange(half_width, dtype=jnp.float32) * 2.0 / values_in.shape[-1])
    angles = positions.astype(jnp.float32)[:, None] * inverse[None, :]
    cosine = jnp.cos(angles)[:, None, :]
    sine_part = jnp.sin(angles)[:, None, :]
    first_half = values_in[..., :half_width]
    second_half = values_in[..., half_width:]
    return jnp.concatenate(
        [
            first_half * cosine - second_half * sine_part,
            second_half * cosine + first_half * sine_part,
        ],
        axis=-1,
    )


def absorb(state, queries, positions, key_block, value_block, first_key):
    running_max, weight_sum, weighted = state
    head_count = weighted.shape[0]
    block_rows = key_block.shape[0]
    scores = jnp.einsum("qgd,kgd->gqk", queries, key_block, preferred_element_type=jnp.float32)
    scores = scores * queries.shape[-1] ** (-0.5)
    key_places = first_key + jnp.arange(block_rows, dtype=jnp.int32)
    allowed = key_places[None, :] <= positions[:, None]
    scores = jnp.where(allowed[None], scores, MASKED)
    scores = scores.reshape(head_count, 2, positions.shape[0], block_rows)
    raised = jnp.maximum(running_max, jnp.max(scores, axis=3))
    factor = jnp.exp(running_max - raised)
    lifted = jnp.exp(scores - raised[..., None])
    weight_sum = factor * weight_sum + jnp.sum(lifted, axis=3)
    values_here = value_block.reshape(block_rows, head_count, -1)
    weighted = factor[..., None] * weighted + jnp.einsum(
        "hjqk,khe->hjqe",
        lifted.astype(jnp.bfloat16),
        values_here,
        preferred_element_type=jnp.float32,
    )
    return (raised, weight_sum, weighted)


def empty_state(head_count, rows, head_width):
    return (
        jnp.full((head_count, 2, rows), MASKED, jnp.float32),
        jnp.zeros((head_count, 2, rows), jnp.float32),
        jnp.zeros((head_count, 2, rows, 2 * head_width), jnp.float32),
    )


def finish(state, lambdas, head_gain):
    running_max, weight_sum, weighted = state
    head_count = weighted.shape[0]
    rows = weighted.shape[2]
    normalized = weighted / weight_sum[..., None]
    difference = normalized[:, 0] - lambdas[:, None, None] * normalized[:, 1]
    scale_back = lax.rsqrt(jnp.mean(difference * difference, axis=2, keepdims=True) + NORM_EPS)
    attended = (difference * scale_back * head_gain[None, None, :] * HEAD_KEEP).astype(jnp.bfloat16)
    attended = jnp.transpose(attended, (1, 0, 2)).reshape(rows, head_count * weighted.shape[3])
    row_lse = jnp.transpose(running_max + jnp.log(weight_sum), (2, 0, 1)).reshape(
        rows, 2 * head_count
    )
    return (attended, row_lse)


def make_fold(groups, row_count, carry, pieces):
    key_piece, value_piece = pieces
    block_rows = min(key_piece.shape[0], row_count)
    shard_count = key_piece.shape[0] // block_rows

    def one_shard(inner_states, shard_index):
        first_key = shard_index * block_rows
        key_block = lax.dynamic_slice_in_dim(key_piece, shard_index * block_rows, block_rows, 0)
        value_block = lax.dynamic_slice_in_dim(value_piece, shard_index * block_rows, block_rows, 0)
        updated_states = []
        for given_state, group in zip(inner_states, groups):
            group_queries, group_places, group_last = group

            def take_block(given):
                return absorb(given, group_queries, group_places, key_block, value_block, first_key)

            def leave_block(given):
                return given

            updated_states.append(
                lax.cond(first_key < group_last, take_block, leave_block, given_state)
            )
        return (tuple(updated_states), None)

    carry, _ = lax.scan(one_shard, carry, jnp.arange(shard_count, dtype=jnp.int32))
    return carry


def per_device(
    tokens,
    norm_gain,
    w_query,
    w_key,
    w_value,
    w_outer,
    w_inner,
    w_signal,
    conv_taps,
    lambdas,
    head_gain,
    attend_proj,
    convolve_proj,
):
    row_count = tokens.shape[0]
    model_width = norm_gain.shape[0]
    head_count = lambdas.shape[0]
    head_width = w_query.shape[1] // (2 * head_count)
    projections = (w_query, w_key, w_value, w_outer, w_inner, w_signal)
    widened = lax.all_gather(tokens, "tp", axis=1, tiled=True).astype(jnp.float32)
    scaled = (widened * norm_gain[None, :]).astype(jnp.bfloat16)
    squares = jnp.sum(widened * widened, axis=1)
    sums = tuple(
        (jnp.dot(scaled, weight, preferred_element_type=jnp.float32) for weight in projections)
    )
    folded = (squares,) + sums
    inv_rms = lax.rsqrt(folded[0] / model_width + NORM_EPS)[:, None]
    offset = lax.axis_index("sp") * row_count
    positions = offset + jnp.arange(row_count, dtype=jnp.int32)
    queries = rotate(
        (inv_rms * folded[1]).reshape(row_count, 2 * head_count, head_width), positions
    ).astype(jnp.bfloat16)
    key_rows = rotate(
        (inv_rms * folded[2]).reshape(row_count, 2 * head_count, head_width), positions
    ).astype(jnp.bfloat16)
    value_rows = (inv_rms * folded[3]).astype(jnp.bfloat16)
    outer_gate = inv_rms * folded[4]
    product = inv_rms * folded[5] * (inv_rms * folded[6])
    half_rows = row_count // 2
    bit_count = lax.axis_size("sp").bit_length() - 1
    handed = queries[half_rows:]
    for bit_index in range(bit_count):
        handed = partner(handed, "sp", bit_index)
    mirror = lax.axis_size("sp") - 1 - lax.axis_index("sp")
    mirror_start = mirror * row_count + half_rows
    mirror_places = mirror_start + jnp.arange(half_rows, dtype=jnp.int32)
    groups = (
        (queries[:half_rows], positions[:half_rows], offset + half_rows),
        (handed, mirror_places, mirror_start + half_rows),
    )
    initial = (
        empty_state(head_count, half_rows, head_width),
        empty_state(head_count, half_rows, head_width),
    )
    states = make_fold(
        groups,
        row_count,
        initial,
        (
            lax.all_gather(key_rows, "sp", axis=0, tiled=True),
            lax.all_gather(value_rows, "sp", axis=0, tiled=True),
        ),
    )
    own_attended, own_lse = finish(states[0], lambdas, head_gain)
    answer = finish(states[1], lambdas, head_gain)
    for bit_index in range(bit_count):
        answer = (
            partner(answer[0], "sp", bit_index),
            partner(answer[1].astype(jnp.bfloat16), "sp", bit_index).astype(jnp.float32),
        )
    attended = jnp.concatenate([own_attended, answer[0]], axis=0)
    row_lse = jnp.concatenate([own_lse, answer[1]], axis=0)
    border = passed_along(product[row_count - 2 :], "sp", 1)
    padded = jnp.concatenate([border, product], axis=0)
    tap_values = conv_taps.astype(jnp.float32)
    smoothed = (
        tap_values[0] * padded[:-2] + tap_values[1] * padded[1:-1] + tap_values[2] * padded[2:]
    )
    convolved = (outer_gate * smoothed).astype(jnp.bfloat16)
    mixed = lax.psum_scatter(
        (
            jnp.dot(attended, attend_proj, preferred_element_type=jnp.float32)
            + jnp.dot(convolved, convolve_proj, preferred_element_type=jnp.float32)
        ).astype(jnp.bfloat16),
        "tp",
        scatter_dimension=0,
        tiled=True,
    )
    return (mixed, row_lse)


def solution(mesh):
    return jax.shard_map(
        per_device,
        mesh=mesh,
        in_specs=(
            P("sp", "tp"),
            P(),
            P(None, "tp"),
            P(None, "tp"),
            P(None, "tp"),
            P(None, "tp"),
            P(None, "tp"),
            P(None, "tp"),
            P(None, "tp"),
            P("tp"),
            P(),
            P("tp", None),
            P("tp", None),
        ),
        out_specs=(P(("sp", "tp"), None), P("sp", "tp")),
        check_vma=False,
    )
```

profile of v0, /device:TPU:0, one launch (start us, length us, event | category | flops | bytes accessed | tf_op | source)
XLA Modules:
  0.0 576.9 jit_solution(11186875485506537824)
XLA Ops:
  10.4 30.4 %all-gather.4.cloned.1.call-done = bf16[768,2048]{1,0:T(8,128)(2,1)} async-done(((bf16[768,512]{1,0:T(8,128)(2,1)}), bf16[768,2048]{1,0:T(8,128)(2,1)}) %all-gather.4.cloned.1.call-update) | async-done | bytes 3145744 | tf_op jit(solution)/shard_map/all_gather | solution.py:134
  43.6 3.4 convolution_multiply_fusion.1
  52.6 4.4 convolution_multiply_fusion
  62.4 4.6 add_convert_fusion.1
  68.5 5.3 multiply_convert_fusion
  77.1 17.9 %collective-permute-done = bf16[384,4,128]{2,0,1:T(8,128)(2,1)S(1)} collective-permute-done((bf16[384,4,128]{2,0,1:T(8,128)(2,1)S(1)}, bf16[384,4,128]{2,0,1:T(8,128)(2,1)S(1)}, u32[]{:S(2)}, u32[]{:S(2)}) %collective-permute-start) | collective-permute-done | bytes 393248 | tf_op jit(solution)/shard_map/ppermute | solution.py:13
  96.5 19.6 %collective-permute-done.1 = bf16[384,4,128]{2,0,1:T(8,128)(2,1)S(1)} collective-permute-done((bf16[384,4,128]{2,0,1:T(8,128)(2,1)S(1)}, bf16[384,4,128]{2,0,1:T(8,128)(2,1)S(1)}, u32[]{:S(2)}, u32[]{:S(2)}) %collective-permute-start.1) | collective-permute-done | bytes 393248 | tf_op jit(solution)/shard_map/ppermute | solution.py:13
  117.0 44.2 %collective-permute-done.2 = bf16[384,4,128]{2,0,1:T(8,128)(2,1)} collective-permute-done((bf16[384,4,128]{2,0,1:T(8,128)(2,1)S(1)}, bf16[384,4,128]{2,0,1:T(8,128)(2,1)}, u32[]{:S(2)}, u32[]{:S(2)}) %collective-permute-start.2) | collective-permute-done | bytes 393248 | tf_op jit(solution)/shard_map/ppermute | solution.py:13
  161.1 25.6 %all-gather.6.cloned.1.call-done = bf16[6144,4,128]{2,0,1:T(8,128)(2,1)} async-done(((bf16[768,4,128]{2,0,1:T(8,128)(2,1)}), bf16[6144,4,128]{2,0,1:T(8,128)(2,1)}) %all-gather.6.cloned.1.call-update) | async-done | bytes 6291472 | tf_op jit(solution)/shard_map/all_gather | solution.py:174
  186.7 100.4 %all-gather.8.cloned.1.call-done = bf16[6144,512]{0,1:T(8,128)(2,1)} async-done(((bf16[768,512]{0,1:T(8,128)(2,1)}), bf16[6144,512]{0,1:T(8,128)(2,1)}) %all-gather.8.cloned.1.call-update) | async-done | bytes 6291472 | tf_op jit(solution)/shard_map/all_gather | solution.py:175
  289.8 182.3 %while.21 = (s32[]{:T(128)}, f32[2,2,384]{2,1,0:T(2,128)S(1)}, f32[2,2,384]{2,1,0:T(2,128)S(1)}, f32[2,2,384,256]{3,2,1,0:T(8,128)}, f32[2,2,384]{2,1,0:T(2,128)...) while((s32[]{:T(128)}, f32[2,2,384]{2,1,0:T(2,128)S(1)}, ...), condition=%wide.region_10.11_spmd.clone, body=%wide.region_1.10_spmd.clone.sunk | while | flops 1830625152 | bytes 47869972 | solution.py:110
  296.6 14.2 %conditional.7 = ((f32[2,2,384]{2,1,0:T(2,128)S(1)}, f32[2,2,384]{2,1,0:T(2,128)S(1)}, f32[2,2,384,256]{3,2,1,0:T(8,128)})) conditional(s32[]{:T(128)} %convert_element_type.122, (f32[2,2,384]{2,1,0:T(2,128)S(1)}, f32[2,2,384]{2,1,0:T(2,128)S(1)}, f32[2,2,384,256]{3,2,1,0:T(8,128)}) %tuple.68, (s32[]{:T(128)}, s32[]{:T(128)}, ...), branch_computations={%region_6.6_spmd, %region_7.9_spmd} | conditional | flops 915312768 | bytes 21576232 | solution.py:106
  296.8 4.4 fusion.44
  305.6 5.2 multiply_add_fusion.2
  310.8 14.1 %conditional.6 = ((f32[2,2,384]{2,1,0:T(2,128)S(1)}, f32[2,2,384]{2,1,0:T(2,128)S(1)}, f32[2,2,384,256]{3,2,1,0:T(8,128)})) conditional(s32[]{:T(128)} %convert_element_type.121, (f32[2,2,384]{2,1,0:T(2,128)S(1)}, f32[2,2,384]{2,1,0:T(2,128)S(1)}, f32[2,2,384,256]{3,2,1,0:T(8,128)}) %tuple.66, (s32[]{:T(128)}, s32[384]{0:T(512)S(1)}, ...), branch_computations={%region_2.2_spmd, %region_3.5_spmd} | conditional | flops 915312384 | bytes 21573156 | solution.py:106
  311.1 4.2 fusion.43
  315.3 3.3 exponential_reduce_fusion
  319.7 5.2 multiply_add_fusion
  331.7 14.2 %conditional.7 = ((f32[2,2,384]{2,1,0:T(2,128)S(1)}, f32[2,2,384]{2,1,0:T(2,128)S(1)}, f32[2,2,384,256]{3,2,1,0:T(8,128)})) conditional(s32[]{:T(128)} %convert_element_type.122, (f32[2,2,384]{2,1,0:T(2,128)S(1)}, f32[2,2,384]{2,1,0:T(2,128)S(1)}, f32[2,2,384,256]{3,2,1,0:T(8,128)}) %tuple.68, (s32[]{:T(128)}, s32[]{:T(128)}, ...), branch_computations={%region_6.6_spmd, %region_7.9_spmd} | conditional | flops 915312768 | bytes 21576232 | solution.py:106
  331.9 4.4 fusion.44
  336.3 3.3 exponential_reduce_fusion.1
  340.7 5.2 multiply_add_fusion.2
  352.7 14.2 %conditional.7 = ((f32[2,2,384]{2,1,0:T(2,128)S(1)}, f32[2,2,384]{2,1,0:T(2,128)S(1)}, f32[2,2,384,256]{3,2,1,0:T(8,128)})) conditional(s32[]{:T(128)} %convert_element_type.122, (f32[2,2,384]{2,1,0:T(2,128)S(1)}, f32[2,2,384]{2,1,0:T(2,128)S(1)}, f32[2,2,384,256]{3,2,1,0:T(8,128)}) %tuple.68, (s32[]{:T(128)}, s32[]{:T(128)}, ...), branch_computations={%region_6.6_spmd, %region_7.9_spmd} | conditional | flops 915312768 | bytes 21576232 | solution.py:106
  353.0 4.4 fusion.44
  361.7 5.2 multiply_add_fusion.2
  373.7 14.2 %conditional.7 = ((f32[2,2,384]{2,1,0:T(2,128)S(1)}, f32[2,2,384]{2,1,0:T(2,128)S(1)}, f32[2,2,384,256]{3,2,1,0:T(8,128)})) conditional(s32[]{:T(128)} %convert_element_type.122, (f32[2,2,384]{2,1,0:T(2,128)S(1)}, f32[2,2,384]{2,1,0:T(2,128)S(1)}, f32[2,2,384,256]{3,2,1,0:T(8,128)}) %tuple.68, (s32[]{:T(128)}, s32[]{:T(128)}, ...), branch_computations={%region_6.6_spmd, %region_7.9_spmd} | conditional | flops 915312768 | bytes 21576232 | solution.py:106
  374.0 4.4 fusion.44
  382.8 5.2 multiply_add_fusion.2
  394.8 14.2 %conditional.7 = ((f32[2,2,384]{2,1,0:T(2,128)S(1)}, f32[2,2,384]{2,1,0:T(2,128)S(1)}, f32[2,2,384,256]{3,2,1,0:T(8,128)})) conditional(s32[]{:T(128)} %convert_element_type.122, (f32[2,2,384]{2,1,0:T(2,128)S(1)}, f32[2,2,384]{2,1,0:T(2,128)S(1)}, f32[2,2,384,256]{3,2,1,0:T(8,128)}) %tuple.68, (s32[]{:T(128)}, s32[]{:T(128)}, ...), branch_computations={%region_6.6_spmd, %region_7.9_spmd} | conditional | flops 915312768 | bytes 21576232 | solution.py:106
  395.0 4.4 fusion.44
  399.4 3.3 exponential_reduce_fusion.1
  403.8 5.2 multiply_add_fusion.2
  415.8 14.2 %conditional.7 = ((f32[2,2,384]{2,1,0:T(2,128)S(1)}, f32[2,2,384]{2,1,0:T(2,128)S(1)}, f32[2,2,384,256]{3,2,1,0:T(8,128)})) conditional(s32[]{:T(128)} %convert_element_type.122, (f32[2,2,384]{2,1,0:T(2,128)S(1)}, f32[2,2,384]{2,1,0:T(2,128)S(1)}, f32[2,2,384,256]{3,2,1,0:T(8,128)}) %tuple.68, (s32[]{:T(128)}, s32[]{:T(128)}, ...), branch_computations={%region_6.6_spmd, %region_7.9_spmd} | conditional | flops 915312768 | bytes 21576232 | solution.py:106
  416.0 4.4 fusion.44
  424.8 5.2 multiply_add_fusion.2
  436.8 14.2 %conditional.7 = ((f32[2,2,384]{2,1,0:T(2,128)S(1)}, f32[2,2,384]{2,1,0:T(2,128)S(1)}, f32[2,2,384,256]{3,2,1,0:T(8,128)})) conditional(s32[]{:T(128)} %convert_element_type.122, (f32[2,2,384]{2,1,0:T(2,128)S(1)}, f32[2,2,384]{2,1,0:T(2,128)S(1)}, f32[2,2,384,256]{3,2,1,0:T(8,128)}) %tuple.68, (s32[]{:T(128)}, s32[]{:T(128)}, ...), branch_computations={%region_6.6_spmd, %region_7.9_spmd} | conditional | flops 915312768 | bytes 21576232 | solution.py:106
  437.1 4.4 fusion.44
  445.8 5.2 multiply_add_fusion.2
  457.8 14.2 %conditional.7 = ((f32[2,2,384]{2,1,0:T(2,128)S(1)}, f32[2,2,384]{2,1,0:T(2,128)S(1)}, f32[2,2,384,256]{3,2,1,0:T(8,128)})) conditional(s32[]{:T(128)} %convert_element_type.122, (f32[2,2,384]{2,1,0:T(2,128)S(1)}, f32[2,2,384]{2,1,0:T(2,128)S(1)}, f32[2,2,384,256]{3,2,1,0:T(8,128)}) %tuple.68, (s32[]{:T(128)}, s32[]{:T(128)}, ...), branch_computations={%region_6.6_spmd, %region_7.9_spmd} | conditional | flops 915312768 | bytes 21576232 | solution.py:106
  458.1 4.4 fusion.44
  466.9 5.2 multiply_add_fusion.2
  485.1 6.3 %collective-permute-done.3 = bf16[384,512]{0,1:T(8,128)(2,1)S(1)} collective-permute-done((bf16[384,512]{0,1:T(8,128)(2,1)S(1)}, bf16[384,512]{0,1:T(8,128)(2,1)S(1)}, u32[]{:S(2)}, u32[]{:S(2)}) %collective-permute-start.3) | collective-permute-done | bytes 393248 | tf_op jit(solution)/shard_map/ppermute | solution.py:13
  496.5 3.7 collective-permute-done.4
  503.3 11.7 %fusion.25 = f32[768,2048]{1,0:T(8,128)} fusion(bf16[512,2048]{1,0:T(8,128)(2,1)S(1)} %copy-done, f32[2,512]{0,1:T(8,128)} %copy-done.10, f32[768,512]{0,1:T(8,128)} %copy-done.4, bf16[2048,512]{1,0:T(8,128)(2,1)} %param.24, bf16[768,2048]{1,0:T(8,128)(2,1)} %all-gather.4.cloned.1.call-done, f32[2048]{0:T(1024)S(1)} %copy-done.11, f32[512]{0:T(512)S(1)} %bitcast.84, ...), kind=kOutput, calls=%fused_computation.50 | convolution fusion | flops 3229876224 | bytes 15225856 | tf_op jit(solution)/shard_map/dot_general | solution.py:197
  518.3 7.1 %add_convert_fusion = bf16[768,2048]{1,0:T(8,128)(2,1)} fusion(f32[768,2048]{1,0:T(8,128)} %fusion.25, bf16[512,2048]{1,0:T(8,128)(2,1)} %param.30, bf16[384,512]{0,1:T(8,128)(2,1)} %collective-permute-done.5, bf16[384,512]{0,1:T(8,128)(2,1)S(1)} %bitcast.80), kind=kOutput, calls=%fused_computation.30 | convolution fusion | flops 1615331328 | bytes 12320768 | tf_op jit(solution)/shard_map/dot_general | solution.py:196
  529.1 6.8 %collective-permute-start.8 = (bf16[384,4]{0,1:T(4,128)(2,1)S(1)}, bf16[384,4]{0,1:T(4,128)(2,1)S(1)}, u32[]{:S(2)}, u32[]{:S(2)}) collective-permute-start(bf16[384,4]{0,1:T(4,128)(2,1)S(1)} %collective-permute-done.7), channel_id=1, source_target_pairs={{0,8},{4,12},{8,0},{12,4},{16,24},{20,28},{24,16},{28,20},{1,9},{5... | collective-permute-start | bytes 9224 | tf_op jit(solution)/shard_map/ppermute | solution.py:13
  537.4 5.5 collective-permute-start.9
  545.2 25.2 %reduce-scatter.2.cloned.1.call-done = bf16[192,2048]{1,0:T(8,128)(2,1)} async-done(((bf16[768,2048]{1,0:T(8,128)(2,1)}), bf16[192,2048]{1,0:T(8,128)(2,1)}) %reduce-scatter.2.cloned.1.call-update) | async-done | bytes 786448 | tf_op jit(solution)/shard_map/reduce_scatter | solution.py:194
  (228 shorter events, 139.7 us)
Async XLA Ops:
  7.2 496.2 %copy-start = (bf16[512,2048]{1,0:T(8,128)(2,1)S(1)}, bf16[512,2048]{1,0:T(8,128)(2,1)}, u32[]{:S(2)}) copy-start(bf16[512,2048]{1,0:T(8,128)(2,1)} %param.31) | copy-start | bytes 6291460
  7.2 33.6 %all-gather.4.cloned.1.call-start = ((), (), s32[]{:S(2)}) async-start(), calls=%async_computation.1 | async-start | bytes 3932160 | tf_op jit(solution)/shard_map/all_gather | solution.py:134
  7.9 35.6 %copy-start.11 = (f32[2048]{0:T(1024)S(1)}, f32[2048]{0:T(1024)}, u32[]{:S(2)}) copy-start(f32[2048]{0:T(1024)} %param.20) | copy-start | bytes 24580
  7.9 178.8 %all-gather.6.cloned.1.call-start = ((), (), s32[]{:S(2)}) async-start(), calls=%async_computation.2 | async-start | bytes 7077888 | tf_op jit(solution)/shard_map/all_gather | solution.py:174
  40.8 2.8 copy-start.2
  68.5 218.7 %all-gather.8.cloned.1.call-start = ((), (), s32[]{:S(2)}) async-start(), calls=%async_computation.3 | async-start | bytes 7077888 | tf_op jit(solution)/shard_map/all_gather | solution.py:175
  73.8 496.6 %reduce-scatter.2.cloned.1.call-start = ((), (), s32[]{:S(2)}) async-start(), calls=%async_computation.4 | async-start | bytes 3932160 | tf_op jit(solution)/shard_map/reduce_scatter | solution.py:194
  75.6 19.4 %collective-permute-start = (bf16[384,4,128]{2,0,1:T(8,128)(2,1)S(1)}, bf16[384,4,128]{2,0,1:T(8,128)(2,1)S(1)}, u32[]{:S(2)}, u32[]{:S(2)}) collective-permute-start(bf16[384,4,128]{2,0,1:T(8,128)(2,1)S(1)} %get-tuple-element.283), channel_id=1, source_target_pairs={{0,4},{4,0},{8,12},{12,8},{16,20},{20,16},{24,28},{28,24},{1,5},{5... | collective-permute-start | bytes 1179656 | tf_op jit(solution)/shard_map/ppermute | solution.py:13
  95.1 21.1 %collective-permute-start.1 = (bf16[384,4,128]{2,0,1:T(8,128)(2,1)S(1)}, bf16[384,4,128]{2,0,1:T(8,128)(2,1)S(1)}, u32[]{:S(2)}, u32[]{:S(2)}) collective-permute-start(bf16[384,4,128]{2,0,1:T(8,128)(2,1)S(1)} %collective-permute-done), channel_id=1, source_target_pairs={{0,8},{4,12},{8,0},{12,4},{16,24},{20,28},{24,16},{28,20},{1,9},{5... | collective-permute-start | bytes 1179656 | tf_op jit(solution)/shard_map/ppermute | solution.py:13
  116.1 45.0 %collective-permute-start.2 = (bf16[384,4,128]{2,0,1:T(8,128)(2,1)S(1)}, bf16[384,4,128]{2,0,1:T(8,128)(2,1)}, u32[]{:S(2)}, u32[]{:S(2)}) collective-permute-start(bf16[384,4,128]{2,0,1:T(8,128)(2,1)S(1)} %collective-permute-done.1), channel_id=1, source_target_pairs={{0,16},{4,20},{8,24},{12,28},{16,0},{20,4},{24,8},{28,12},{1,17},{... | collective-permute-start | bytes 1179656 | tf_op jit(solution)/shard_map/ppermute | solution.py:13
  478.1 1.9 copy-start.1
  480.0 0.7 copy-start.6
  480.7 0.7 copy-start.7
  480.7 1.6 copy-start.8
  481.0 2.3 copy-start.3
  481.7 10.1 %copy-start.9 = (bf16[2048,512]{1,0:T(8,128)(2,1)S(1)}, bf16[2048,512]{1,0:T(8,128)(2,1)}, u32[]{:S(2)}) copy-start(bf16[2048,512]{1,0:T(8,128)(2,1)} %param.26) | copy-start | bytes 6291460
  481.7 9.7 %collective-permute-start.3 = (bf16[384,512]{0,1:T(8,128)(2,1)S(1)}, bf16[384,512]{0,1:T(8,128)(2,1)S(1)}, u32[]{:S(2)}, u32[]{:S(2)}) collective-permute-start(bf16[384,512]{0,1:T(8,128)(2,1)S(1)} %bitcast.81), channel_id=1, source_target_pairs={{0,4},{4,0},{8,12},{12,8},{16,20},{20,16},{24,28},{28,24},{1,5},{5... | collective-permute-start | bytes 1179656 | tf_op jit(solution)/shard_map/ppermute | solution.py:13
  485.1 11.3 %copy-start.5 = (bf16[3,512]{1,0:T(4,128)(2,1)S(1)}, bf16[3,512]{1,0:T(4,128)(2,1)}, u32[]{:S(2)}) copy-start(bf16[3,512]{1,0:T(4,128)(2,1)} %param.27) | copy-start | bytes 9220
  491.4 8.8 %collective-permute-start.4 = (bf16[384,512]{0,1:T(8,128)(2,1)S(1)}, bf16[384,512]{0,1:T(8,128)(2,1)S(1)}, u32[]{:S(2)}, u32[]{:S(2)}) collective-permute-start(bf16[384,512]{0,1:T(8,128)(2,1)S(1)} %collective-permute-done.3), channel_id=1, source_target_pairs={{0,8},{4,12},{8,0},{12,4},{16,24},{20,28},{24,16},{28,20},{1,9},{5... | collective-permute-start | bytes 1179656 | tf_op jit(solution)/shard_map/ppermute | solution.py:13
  493.7 8.9 %copy-start.4 = (f32[768,512]{0,1:T(8,128)}, f32[768,512]{0,1:T(8,128)S(1)}, u32[]{:S(2)}) copy-start(f32[768,512]{0,1:T(8,128)S(1)} %multiply_multiply_fusion) | copy-start | bytes 4718596
  493.8 8.8 %collective-permute-start.6 = (f32[2,512]{0,1:T(8,128)S(1)}, f32[2,512]{0,1:T(8,128)S(1)}, u32[]{:S(2)}, u32[]{:S(2)}) collective-permute-start(f32[2,512]{0,1:T(8,128)S(1)} %slice.79), channel_id=1, source_target_pairs={{0,4},{4,8},{8,12},{12,16},{16,20},{20,24},{24,28},{1,5},{5,9},{9,... | collective-permute-start | bytes 12296 | tf_op jit(solution)/shard_map/ppermute | solution.py:19
  500.2 18.0 %collective-permute-start.5 = (bf16[384,512]{0,1:T(8,128)(2,1)S(1)}, bf16[384,512]{0,1:T(8,128)(2,1)}, u32[]{:S(2)}, u32[]{:S(2)}) collective-permute-start(bf16[384,512]{0,1:T(8,128)(2,1)S(1)} %collective-permute-done.4), channel_id=1, source_target_pairs={{0,16},{4,20},{8,24},{12,28},{16,0},{20,4},{24,8},{28,12},{1,17},{... | collective-permute-start | bytes 1179656 | tf_op jit(solution)/shard_map/ppermute | solution.py:13
  502.6 0.7 copy-start.10
  525.4 3.7 collective-permute-start.7
  529.1 8.4 %collective-permute-start.8 = (bf16[384,4]{0,1:T(4,128)(2,1)S(1)}, bf16[384,4]{0,1:T(4,128)(2,1)S(1)}, u32[]{:S(2)}, u32[]{:S(2)}) collective-permute-start(bf16[384,4]{0,1:T(4,128)(2,1)S(1)} %collective-permute-done.7), channel_id=1, source_target_pairs={{0,8},{4,12},{8,0},{12,4},{16,24},{20,28},{24,16},{28,20},{1,9},{5... | collective-permute-start | bytes 9224 | tf_op jit(solution)/shard_map/ppermute | solution.py:13
  537.4 7.1 %collective-permute-start.9 = (bf16[384,4]{0,1:T(4,128)(2,1)S(1)}, bf16[384,4]{0,1:T(4,128)(2,1)S(1)}, u32[]{:S(2)}, u32[]{:S(2)}) collective-permute-start(bf16[384,4]{0,1:T(4,128)(2,1)S(1)} %collective-permute-done.8), channel_id=1, source_target_pairs={{0,16},{4,20},{8,24},{12,28},{16,0},{20,4},{24,8},{28,12},{1,17},{... | collective-permute-start | bytes 9224 | tf_op jit(solution)/shard_map/ppermute | solution.py:13
Sparse Core Ops, SparseCore 0:
  9.5 31.2 all-gather.3
  68.6 118.1 all-gather.5
  189.0 98.1 all-gather.7
  525.5 44.8 reduce-scatter.1
where the time goes:
time: 579 us; the launch traced here: 577 us
  waiting for transfers between devices  284 us (49%)
  matrix products  121 us (21%)
  local copies, waits for them, and re-layouts  82 us (14%)
  other arithmetic  47.7 us (8%)
  starting transfers between devices  22.8 us (4%)
  between operations  14 us (2%)
    ppermute x9, waiting for transfers between devices, partner(): lax.ppermute(value, axis, [(i, i ^ 1 << stride) for i in range(lax.axis_s...  101 us
    all_gather x1, waiting for transfers between devices, per_device(): lax.all_gather(value_rows, 'sp', axis=0, tiled=True)  100 us
    dot_general x9, matrix products, absorb(): jnp.einsum('hjqk,khe->hjqe', lifted.astype(jnp.bfloat16), values_here, pr...  46.7 us
    dot_general x9, matrix products, absorb(): jnp.einsum('qgd,kgd->gqk', queries, key_block, preferred_element_type=jnp...  39.1 us
    all_gather x1, waiting for transfers between devices, per_device(): lax.all_gather(tokens, 'tp', axis=1, tiled=True).astype(jnp.float32)  30.4 us
    reduce_sum x9, other arithmetic, absorb(): weight_sum = factor * weight_sum + jnp.sum(lifted, axis=3)  29.5 us
    dynamic_slice x16, local copies, waits for them, and re-layouts, one_shard(): lax.dynamic_slice_in_dim(value_piece, shard_index * block_rows, block_row...  27.8 us
    all_gather x1, waiting for transfers between devices, per_device(): lax.all_gather(key_rows, 'sp', axis=0, tiled=True)  25.6 us
  transfers between devices with their start and end apart: 14, of which 13 were waited for; matrix products, arithmetic and copies ran while one was open for 4% of the time, Pallas kernels for 0%

commit v1 on v0

--- a/solution.py
+++ b/solution.py
@@ -1,12 +1,19 @@
+import functools
+import math
+
 import jax
 import jax.numpy as jnp
 from jax import lax
+from jax.experimental import pallas as pl
+from jax.experimental.pallas import tpu as pltpu
 from jax.sharding import PartitionSpec as P
 
 ROPE_BASE = 500000.0
 NORM_EPS = 1e-05
 HEAD_KEEP = 0.8
 MASKED = -1e30
+LOG2E = math.log2(math.e)
+MESH = pl.DeviceIdType.MESH
 
 
 def partner(value, axis, stride):
@@ -83,6 +90,363 @@
     return (attended, row_lse)
 
 
+def project_kernel(scale, tok_ref, gain_ref, wq_ref, wk_ref, wv_ref, cos_ref, sin_ref, q_ref, kv_ref):
+    heads, _, pair = q_ref.shape
+    width = pair // 2
+    widened = tok_ref[...].astype(jnp.float32)
+    scaled = (widened * gain_ref[...]).astype(jnp.bfloat16)
+    mean = jnp.sum(widened * widened, axis=1, keepdims=True) / widened.shape[1]
+    inv_rms = lax.rsqrt(mean + NORM_EPS)
+    cosine, sine = cos_ref[...], sin_ref[...]
+
+    def rotary(x):
+        return x * cosine + pltpu.roll(x, width // 2, 1) * sine
+
+    q = jnp.dot(scaled, wq_ref[...], preferred_element_type=jnp.float32) * inv_rms
+    k = jnp.dot(scaled, wk_ref[...], preferred_element_type=jnp.float32) * inv_rms
+    v = jnp.dot(scaled, wv_ref[...], preferred_element_type=jnp.float32) * inv_rms
+    for head in range(heads):
+        for j in range(2):
+            cols = slice((2 * head + j) * width, (2 * head + j + 1) * width)
+            place = slice(j * width, (j + 1) * width)
+            q_ref[head, :, place] = (rotary(q[:, cols]) * scale).astype(jnp.bfloat16)
+            kv_ref[head, :, place] = rotary(k[:, cols]).astype(jnp.bfloat16)
+        kv_ref[head, :, pair:] = v[:, head * pair : (head + 1) * pair].astype(jnp.bfloat16)
+
+
+def project(tokens, norm_gain, w_query, w_key, w_value, positions, head_count, head_width):
+    rows, model_width = tokens.shape
+    half = head_width // 2
+    inverse = ROPE_BASE ** (-jnp.arange(half, dtype=jnp.float32) * 2.0 / head_width)
+    angles = positions.astype(jnp.float32)[:, None] * inverse[None, :]
+    cosine, sine = jnp.cos(angles), jnp.sin(angles)
+    cosine = jnp.concatenate([cosine, cosine], axis=1)
+    sine = jnp.concatenate([-sine, sine], axis=1)
+    pair = 2 * head_width
+    block = rows // 3 if rows % 48 == 0 else rows
+    whole = lambda shape: pl.BlockSpec(shape, lambda i: (0,) * len(shape))
+    return pl.pallas_call(
+        functools.partial(project_kernel, head_width ** (-0.5) * LOG2E),
+        grid=(rows // block,),
+        out_shape=(
+            jax.ShapeDtypeStruct((head_count, rows, pair), jnp.bfloat16),
+            jax.ShapeDtypeStruct((head_count, rows, 2 * pair), jnp.bfloat16),
+        ),
+        in_specs=[
+            pl.BlockSpec((block, model_width), lambda i: (i, 0)),
+            whole((1, model_width)),
+            whole(w_query.shape),
+            whole(w_key.shape),
+            whole(w_value.shape),
+            pl.BlockSpec((block, head_width), lambda i: (i, 0)),
+            pl.BlockSpec((block, head_width), lambda i: (i, 0)),
+        ],
+        out_specs=(
+            pl.BlockSpec((head_count, block, pair), lambda i: (0, i, 0)),
+            pl.BlockSpec((head_count, block, 2 * pair), lambda i: (0, i, 0)),
+        ),
+        compiler_params=pltpu.CompilerParams(vmem_limit_bytes=48 * 2**20),
+        cost_estimate=pl.CostEstimate(
+            flops=6 * rows * model_width * w_query.shape[1],
+            bytes_accessed=2 * (rows * model_width + 3 * w_query.size + 3 * rows * w_query.shape[1]),
+            transcendentals=0,
+        ),
+        name="project_qkv",
+    )(tokens, norm_gain[None, :], w_query, w_key, w_value, cosine, sine)
+
+
+def attend_kernel(
+    groups,
+    block,
+    q_keep,
+    q_recv,
+    kv_keep,
+    kv_recv,
+    lambdas_ref,
+    gain_ref,
+    out_ref,
+    lse_ref,
+    kv_all,
+    q_own,
+    q_far,
+    acc,
+    top,
+    total,
+    local_sem,
+    send_right,
+    send_left,
+    recv_sem,
+    far_send,
+    far_recv,
+):
+    sp = lax.axis_index("sp")
+    tp = lax.axis_index("tp")
+    g, y = sp // 2, sp % 2
+    mirror = groups - 1 - g
+    rows, pair = q_keep.shape
+    width = pair // 2
+    blocks = rows // block
+
+    def at(group):
+        return (2 * group + y, tp)
+
+    loads = (
+        pltpu.make_async_copy(q_keep, q_own.at[y], local_sem.at[0]),
+        pltpu.make_async_copy(q_recv, q_own.at[1 - y], local_sem.at[1]),
+        pltpu.make_async_copy(kv_keep, kv_all.at[sp], local_sem.at[2]),
+        pltpu.make_async_copy(kv_recv, kv_all.at[2 * g + 1 - y], local_sem.at[3]),
+    )
+    for load in loads:
+        load.start()
+    barrier = pltpu.get_barrier_semaphore()
+    for step in range(1, groups):
+        pl.semaphore_signal(
+            barrier, inc=1, device_id=at(lax.rem(g + step, groups)), device_id_type=MESH
+        )
+    pl.semaphore_wait(barrier, groups - 1)
+    for load in loads:
+        load.wait()
+
+    def right(chunk):
+        return pltpu.make_async_remote_copy(
+            src_ref=kv_all.at[chunk],
+            dst_ref=kv_all.at[chunk],
+            send_sem=send_right.at[chunk],
+            recv_sem=recv_sem.at[chunk],
+            device_id=at(jnp.minimum(g + 1, groups - 1)),
+            device_id_type=MESH,
+        )
+
+    def left(chunk):
+        return pltpu.make_async_remote_copy(
+            src_ref=kv_all.at[chunk],
+            dst_ref=kv_all.at[chunk],
+            send_sem=send_left.at[chunk],
+            recv_sem=recv_sem.at[chunk],
+            device_id=at(jnp.maximum(g - 1, 0)),
+            device_id_type=MESH,
+        )
+
+    far = pltpu.make_async_remote_copy(
+        src_ref=q_own.at[1],
+        dst_ref=q_far,
+        send_sem=far_send,
+        recv_sem=far_recv,
+        device_id=at(mirror),
+        device_id_type=MESH,
+    )
+    far.start()
+
+    @pl.when(g < groups - 1)
+    def _():
+        right(2 * g + 1).start()
+        right(2 * g).start()
+
+    @pl.when(g > 0)
+    def _():
+        left(2 * g).start()
+        left(2 * g + 1).start()
+
+    acc[...] = jnp.zeros_like(acc)
+    total[...] = jnp.zeros_like(total)
+    top[...] = jnp.full_like(top, MASKED)
+
+    def update(r, j, start, scores, values):
+        here = pl.ds(start, block)
+        old = top[r, j, here, :]
+        new = jnp.maximum(old, jnp.max(scores, axis=1, keepdims=True))
+        shrink = jnp.exp2(old - new)
+        lifted = jnp.exp2(scores - new[:, :1])
+        top[r, j, here, :] = new
+        total[r, j, here, :] = shrink * total[r, j, here, :] + jnp.sum(lifted, axis=1, keepdims=True)
+        acc[r, j, here, :] = shrink[:, :1] * acc[r, j, here, :] + jnp.dot(
+            lifted.astype(jnp.bfloat16), values, preferred_element_type=jnp.float32
+        )
+
+    def scores_of(r, j, start, chunk, length):
+        cols = slice(j * width, (j + 1) * width)
+        queries = q_use[r, pl.ds(start, block), cols]
+        keys = kv_all[chunk, :length, cols]
+        return lax.dot_general(
+            queries, keys, (((1,), (1,)), ((), ())), preferred_element_type=jnp.float32
+        )
+
+    q_use = q_own
+
+    def process(r, chunk):
+        q_chunk = jnp.where(r == 0, 2 * g, 2 * mirror + 1)
+
+        @pl.when(chunk < q_chunk)
+        def _():
+            def one(b, carry):
+                start = pl.multiple_of(b * block, block)
+                for j in range(2):
+                    update(r, j, start, scores_of(r, j, start, chunk, rows), kv_all[chunk, :, pair:])
+                return carry
+
+            lax.fori_loop(0, blocks, one, 0)
+
+        @pl.when(chunk == q_chunk)
+        def _():
+            for b in range(blocks):
+                length = (b + 1) * block
+                query_at = b * block + lax.broadcasted_iota(jnp.int32, (block, length), 0)
+                key_at = lax.broadcasted_iota(jnp.int32, (block, length), 1)
+                for j in range(2):
+                    scores = scores_of(r, j, b * block, chunk, length)
+                    scores = jnp.where(key_at <= query_at, scores, MASKED)
+                    update(r, j, b * block, scores, kv_all[chunk, :length, pair:])
+
+    far.wait()
+    swap = pltpu.make_async_copy(q_far, q_own.at[1], local_sem.at[0])
+    swap.start()
+    swap.wait()
+
+    def visit(i, carry):
+        step, half, side = i // 4, (i // 2) % 2, i % 2
+        group = jnp.where(side == 0, g - step, g + step)
+        chunk = jnp.where(side == 0, 2 * group + 1 - half, 2 * group + half)
+        exists = jnp.logical_and(group >= 0, group < groups)
+        exists = jnp.logical_and(exists, jnp.logical_or(step > 0, side == 0))
+
+        @pl.when(exists)
+        def _():
+            @pl.when(jnp.logical_and(step > 0, side == 0))
+            def _():
+                right(chunk).wait_recv()
+
+                @pl.when(g < groups - 1)
+                def _():
+                    right(chunk).start()
+
+            @pl.when(jnp.logical_and(step > 0, side == 1))
+            def _():
+                left(chunk).wait_recv()
+
+                @pl.when(g > 0)
+                def _():
+                    left(chunk).start()
+
+            def each(r, inner):
+                process(r, chunk)
+                return inner
+
+            lax.fori_loop(0, 2, each, 0)
+
+        return carry
+
+    lax.fori_loop(0, 4 * groups, visit, 0)
+
+    lam = lambdas_ref[y]
+    gain = gain_ref[...] * HEAD_KEEP
+
+    def close(i, carry):
+        r, start = i // blocks, pl.multiple_of((i % blocks) * block, block)
+        here = pl.ds(start, block)
+        sums = [total[r, j, here, :] for j in range(2)]
+        parts = [acc[r, j, here, :] / sums[j][:, :1] for j in range(2)]
+        difference = parts[0] - lam * parts[1]
+        mean = jnp.mean(difference * difference, axis=1, keepdims=True)
+        out_ref[r, here, :] = (difference * lax.rsqrt(mean + NORM_EPS) * gain).astype(jnp.bfloat16)
+        lses = [top[r, j, here, :] * (1.0 / LOG2E) + jnp.log(sums[j]) for j in range(2)]
+        lane = lax.broadcasted_iota(jnp.int32, lses[0].shape, 1)
+        lse_ref[r, here, :] = jnp.where(lane == 0, lses[0], lses[1])
+        return carry
+
+    lax.fori_loop(0, 2 * blocks, close, 0)
+
+    def drain(chunk, carry):
+        @pl.when(jnp.logical_and(g < groups - 1, chunk < 2 * g + 2))
+        def _():
+            right(chunk).wait_send()
+
+        @pl.when(jnp.logical_and(g > 0, chunk >= 2 * g))
+        def _():
+            left(chunk).wait_send()
+
+        return carry
+
+    lax.fori_loop(0, 2 * groups, drain, 0)
+
+
+def attend(groups, q_keep, q_recv, kv_keep, kv_recv, lambdas, head_gain):
+    rows, pair = q_keep.shape
+    block = rows // 3 if rows % 48 == 0 else rows
+    vmem = pl.BlockSpec(memory_space=pltpu.VMEM)
+    anywhere = pl.BlockSpec(memory_space=pl.ANY)
+    chunks = 2 * groups
+    lanes = 128
+    return pl.pallas_call(
+        functools.partial(attend_kernel, groups, block),
+        out_shape=(
+            jax.ShapeDtypeStruct((2, rows, pair), jnp.bfloat16),
+            jax.ShapeDtypeStruct((2, rows, lanes), jnp.float32),
+        ),
+        in_specs=[anywhere] * 4 + [pl.BlockSpec(memory_space=pltpu.SMEM), vmem],
+        out_specs=(vmem, vmem),
+        scratch_shapes=[
+            pltpu.VMEM((chunks, rows, 2 * pair), jnp.bfloat16),
+            pltpu.VMEM((2, rows, pair), jnp.bfloat16),
+            pltpu.VMEM((rows, pair), jnp.bfloat16),
+            pltpu.VMEM((2, 2, rows, pair), jnp.float32),
+            pltpu.VMEM((2, 2, rows, lanes), jnp.float32),
+            pltpu.VMEM((2, 2, rows, lanes), jnp.float32),
+            pltpu.SemaphoreType.DMA((4,)),
+            pltpu.SemaphoreType.DMA((chunks,)),
+            pltpu.SemaphoreType.DMA((chunks,)),
+            pltpu.SemaphoreType.DMA((chunks,)),
+            pltpu.SemaphoreType.DMA,
+            pltpu.SemaphoreType.DMA,
+        ],
+        compiler_params=pltpu.CompilerParams(
+            collective_id=0, has_side_effects=True, vmem_limit_bytes=56 * 2**20
+        ),
+        cost_estimate=pl.CostEstimate(
+            flops=8 * chunks * rows * rows * 3 * pair // 4,
+            bytes_accessed=8 * rows * pair,
+            transcendentals=0,
+        ),
+        name="attend_line",
+    )(q_keep, q_recv, kv_keep, kv_recv, lambdas, head_gain[None, :])
+
+
+def attention_by_head(tokens, norm_gain, w_query, w_key, w_value, lambdas, head_gain, positions):
+    head_count = lambdas.shape[0]
+    head_width = w_query.shape[1] // (2 * head_count)
+    count = lax.axis_size("sp")
+    groups = count // 2
+    y = lax.axis_index("sp") % 2
+    queries, key_values = project(
+        tokens, norm_gain, w_query, w_key, w_value, positions, head_count, head_width
+    )
+    take = lambda array, index: lax.dynamic_index_in_dim(array, index, 0, keepdims=False)
+    kv_recv = partner(take(key_values, 1 - y), "sp", 0)
+    q_recv = partner(take(queries, 1 - y), "sp", 0)
+    result, lse = attend(
+        groups, take(queries, y), q_recv, take(key_values, y), kv_recv, lambdas, head_gain
+    )
+    lse = lse[:, :, :2]
+    cross = []
+    second = []
+    for group in range(groups):
+        far = 2 * (groups - 1 - group) + 1
+        cross += [(2 * group + 1, 2 * group), (2 * group, far)]
+        second += [(2 * group + 1, far)]
+    mine = jnp.where(y == 1, result[0], result[1])
+    crossed = lax.ppermute(mine, "sp", cross)
+    seconded = lax.ppermute(result[1], "sp", second)
+    crossed_lse = lax.ppermute(jnp.where(y == 1, lse[0], lse[1]), "sp", cross)
+    seconded_lse = lax.ppermute(lse[1], "sp", second)
+    first = jnp.where(y == 0, result[0], crossed)
+    last = jnp.where(y == 0, crossed, seconded)
+    first_lse = jnp.where(y == 0, lse[0], crossed_lse)
+    last_lse = jnp.where(y == 0, crossed_lse, seconded_lse)
+    return (
+        jnp.concatenate([first, last], axis=1),
+        jnp.concatenate([first_lse, last_lse], axis=1),
+    )
+
+
 def make_fold(groups, row_count, carry, pieces):
     key_piece, value_piece = pieces
     block_rows = min(key_piece.shape[0], row_count)
@@ -109,6 +473,52 @@
 
     carry, _ = lax.scan(one_shard, carry, jnp.arange(shard_count, dtype=jnp.int32))
     return carry
+
+
+def attention_by_rows(query_sums, key_sums, value_sums, lambdas, head_gain, positions):
+    row_count = query_sums.shape[0]
+    head_count = lambdas.shape[0]
+    head_width = query_sums.shape[1] // (2 * head_count)
+    offset = lax.axis_index("sp") * row_count
+    split = (row_count, 2 * head_count, head_width)
+    queries = rotate(query_sums.reshape(split), positions).astype(jnp.bfloat16)
+    key_rows = rotate(key_sums.reshape(split), positions).astype(jnp.bfloat16)
+    value_rows = value_sums.astype(jnp.bfloat16)
+    half_rows = row_count // 2
+    bit_count = lax.axis_size("sp").bit_length() - 1
+    handed = queries[half_rows:]
+    for bit_index in range(bit_count):
+        handed = partner(handed, "sp", bit_index)
+    mirror = lax.axis_size("sp") - 1 - lax.axis_index("sp")
+    mirror_start = mirror * row_count + half_rows
+    mirror_places = mirror_start + jnp.arange(half_rows, dtype=jnp.int32)
+    groups = (
+        (queries[:half_rows], positions[:half_rows], offset + half_rows),
+        (handed, mirror_places, mirror_start + half_rows),
+    )
+    initial = (
+        empty_state(head_count, half_rows, head_width),
+        empty_state(head_count, half_rows, head_width),
+    )
+    states = make_fold(
+        groups,
+        row_count,
+        initial,
+        (
+            lax.all_gather(key_rows, "sp", axis=0, tiled=True),
+            lax.all_gather(value_rows, "sp", axis=0, tiled=True),
+        ),
+    )
+    own_attended, own_lse = finish(states[0], lambdas, head_gain)
+    answer = finish(states[1], lambdas, head_gain)
+    for bit_index in range(bit_count):
+        answer = (
+            partner(answer[0], "sp", bit_index),
+            partner(answer[1].astype(jnp.bfloat16), "sp", bit_index).astype(jnp.float32),
+        )
+    attended = jnp.concatenate([own_attended, answer[0]], axis=0)
+    row_lse = jnp.concatenate([own_lse, answer[1]], axis=0)
+    return (attended, row_lse)
 
 
 def per_device(
@@ -130,60 +540,33 @@
     model_width = norm_gain.shape[0]
     head_count = lambdas.shape[0]
     head_width = w_query.shape[1] // (2 * head_count)
-    projections = (w_query, w_key, w_value, w_outer, w_inner, w_signal)
-    widened = lax.all_gather(tokens, "tp", axis=1, tiled=True).astype(jnp.float32)
+    count = lax.axis_size("sp")
+    gathered = lax.all_gather(tokens, "tp", axis=1, tiled=True)
+    widened = gathered.astype(jnp.float32)
     scaled = (widened * norm_gain[None, :]).astype(jnp.bfloat16)
     squares = jnp.sum(widened * widened, axis=1)
-    sums = tuple(
-        (jnp.dot(scaled, weight, preferred_element_type=jnp.float32) for weight in projections)
-    )
-    folded = (squares,) + sums
-    inv_rms = lax.rsqrt(folded[0] / model_width + NORM_EPS)[:, None]
+    inv_rms = lax.rsqrt(squares / model_width + NORM_EPS)[:, None]
     offset = lax.axis_index("sp") * row_count
     positions = offset + jnp.arange(row_count, dtype=jnp.int32)
-    queries = rotate(
-        (inv_rms * folded[1]).reshape(row_count, 2 * head_count, head_width), positions
-    ).astype(jnp.bfloat16)
-    key_rows = rotate(
-        (inv_rms * folded[2]).reshape(row_count, 2 * head_count, head_width), positions
-    ).astype(jnp.bfloat16)
-    value_rows = (inv_rms * folded[3]).astype(jnp.bfloat16)
-    outer_gate = inv_rms * folded[4]
-    product = inv_rms * folded[5] * (inv_rms * folded[6])
-    half_rows = row_count // 2
-    bit_count = lax.axis_size("sp").bit_length() - 1
-    handed = queries[half_rows:]
-    for bit_index in range(bit_count):
-        handed = partner(handed, "sp", bit_index)
-    mirror = lax.axis_size("sp") - 1 - lax.axis_index("sp")
-    mirror_start = mirror * row_count + half_rows
-    mirror_places = mirror_start + jnp.arange(half_rows, dtype=jnp.int32)
-    groups = (
-        (queries[:half_rows], positions[:half_rows], offset + half_rows),
-        (handed, mirror_places, mirror_start + half_rows),
-    )
-    initial = (
-        empty_state(head_count, half_rows, head_width),
-        empty_state(head_count, half_rows, head_width),
-    )
-    states = make_fold(
-        groups,
-        row_count,
-        initial,
-        (
-            lax.all_gather(key_rows, "sp", axis=0, tiled=True),
-            lax.all_gather(value_rows, "sp", axis=0, tiled=True),
-        ),
-    )
-    own_attended, own_lse = finish(states[0], lambdas, head_gain)
-    answer = finish(states[1], lambdas, head_gain)
-    for bit_index in range(bit_count):
-        answer = (
-            partner(answer[0], "sp", bit_index),
-            partner(answer[1].astype(jnp.bfloat16), "sp", bit_index).astype(jnp.float32),
-        )
-    attended = jnp.concatenate([own_attended, answer[0]], axis=0)
-    row_lse = jnp.concatenate([own_lse, answer[1]], axis=0)
+
+    def product_of(weight):
+        return inv_rms * jnp.dot(scaled, weight, preferred_element_type=jnp.float32)
+
+    if head_count == 2 and head_width == 128 and count % 4 == 0:
+        attended, row_lse = attention_by_head(
+            gathered, norm_gain, w_query, w_key, w_value, lambdas, head_gain, positions
+        )
+    else:
+        attended, row_lse = attention_by_rows(
+            product_of(w_query),
+            product_of(w_key),
+            product_of(w_value),
+            lambdas,
+            head_gain,
+            positions,
+        )
+    outer_gate = product_of(w_outer)
+    product = product_of(w_inner) * product_of(w_signal)
     border = passed_along(product[row_count - 2 :], "sp", 1)
     padded = jnp.concatenate([border, product], axis=0)
     tap_values = conv_taps.astype(jnp.float32)

time: 579 us -> 274 us (0.47)
  waiting for transfers between devices: 284 us -> 74.9 us
  Pallas kernels: 0 us -> 128 us
  matrix products: 121 us -> 21 us
  local copies, waits for them, and re-layouts: 82 us -> 7.87 us
  other arithmetic: 47.7 us -> 6.9 us
    pallas_call x0 -> x2, Pallas kernels: none -> 128 us  [the longest x1 120 us: attend(): pl.pallas_call(functools.partial(attend_kernel, groups, block), out_shape...]
    all_gather x3 -> x1, waiting for transfers between devices: 156 us -> 31 us  [per_device(): gathered = lax.all_gather(tokens, 'tp', axis=1, tiled=True)]
    dot_general x23 -> x2, matrix products: 103 us -> 3.6 us  [product_of(): return inv_rms * jnp.dot(scaled, weight, preferred_element_type=jnp.float32)]
    ppermute x9 -> x2, waiting for transfers between devices: 101 us -> 18.3 us  [partner(): lax.ppermute(value, axis, [(i, i ^ 1 << stride) for i in range(lax.axis_s...]
    dynamic_slice x32 -> x0, local copies, waits for them, and re-layouts: 49.1 us -> none  [the longest x16 27.8 us: one_shard(): lax.dynamic_slice_in_dim(value_piece, shard_index * block_rows, block_row...]
    reduce_sum x10 -> x0, other arithmetic: 29.8 us -> none  [the longest x9 29.5 us: absorb(): weight_sum = factor * weight_sum + jnp.sum(lifted, axis=3)]
    ppermute x9 -> x2, starting transfers between devices: 19.9 us -> 2.03 us  [partner(): lax.ppermute(value, axis, [(i, i ^ 1 << stride) for i in range(lax.axis_s...]
    ppermute x0 -> x4, starting transfers between devices: none -> 15.1 us  [the longest x1 6.54 us: attention_by_head(): crossed_lse = lax.ppermute(jnp.where(y == 1, lse[0], lse[1]), 'sp', cross)]
  transfers between devices with their start and end apart: 14 -> 9, of which waited for: 13 -> 5; matrix products, arithmetic and copies ran while one was open for 4% -> 8% of each run, Pallas kernels for 0% -> 44%
where the time goes in v1:
time: 274 us
  Pallas kernels  128 us (47%)
  waiting for transfers between devices  74.9 us (27%)
  matrix products  21 us (8%)
  starting transfers between devices  20.6 us (8%)
  between operations  14.3 us (5%)
  local copies, waits for them, and re-layouts  7.87 us (3%)
  other arithmetic  6.9 us (3%)
    pallas_call x1, Pallas kernels, attend(): pl.pallas_call(functools.partial(attend_kernel, groups, block), out_shape...  120 us
    all_gather x1, waiting for transfers between devices, per_device(): gathered = lax.all_gather(tokens, 'tp', axis=1, tiled=True)  31 us
    ppermute x2, waiting for transfers between devices, partner(): lax.ppermute(value, axis, [(i, i ^ 1 << stride) for i in range(lax.axis_s...  18.3 us
    reduce_scatter x1, waiting for transfers between devices, per_device(): lax.psum_scatter((jnp.dot(attended, attend_proj, preferred_element_type=j...  18.3 us
    dot_general x1, matrix products, per_device(): jnp.dot(convolved, convolve_proj, preferred_element_type=jnp.float32)  10.4 us
    pallas_call x1, Pallas kernels, project(): pl.pallas_call(functools.partial(project_kernel, head_width ** (-0.5) * L...  8.24 us
    dot_general x1, matrix products, per_device(): jnp.dot(attended, attend_proj, preferred_element_type=jnp.float32)  6.98 us
    ppermute x1, starting transfers between devices, attention_by_head(): crossed_lse = lax.ppermute(jnp.where(y == 1, lse[0], lse[1]), 'sp', cross)  6.54 us
  transfers between devices with their start and end apart: 9, of which 5 were waited for; matrix products, arithmetic and copies ran while one was open for 8% of the time, Pallas kernels for 44%

profile of v1, /device:TPU:0, one launch (start us, length us, event | category | flops | bytes accessed | tf_op | source)
XLA Modules:
  0.0 273.7 jit_solution(6467589926281468563)
XLA Ops:
  7.2 0.0 copy-start
  7.2 0.0 copy-start.6
  7.2 0.0 copy-start.2
  7.2 0.0 all-gather.2.cloned.1.call-start
  7.2 0.7 all-gather.2.cloned.1.call-update
  7.9 0.0 reduce-scatter.2.cloned.1.call-start
  8.0 1.4 fusion.29
  9.5 0.3 pad_maximum_fusion.1
  9.8 31.0 %all-gather.2.cloned.1.call-done.tok_ref = bf16[768,2048]{1,0:T(8,128)(2,1)} async-done(((bf16[768,512]{1,0:T(8,128)(2,1)}), bf16[768,2048]{1,0:T(8,128)(2,1)}) %all-gather.2.cloned.1.call-update) | async-done | bytes 3145744 | tf_op jit(solution)/shard_map/all_gather | solution.py:544
  40.8 1.6 copy-done.1
  42.4 8.2 %project_qkv.1 = (bf16[2,768,256]{2,1,0:T(8,128)(2,1)S(1)}, bf16[2,768,512]{2,1,0:T(8,128)(2,1)S(1)}) custom-call(bf16[768,2048]{1,0:T(8,128)(2,1)} %all-gather.2.cloned.1.call-done.tok_ref, f32[1,2048]{1,0:T(1,128)S(1)} %bitcast.32, bf16[2048,512]{1,0:T(8,128)(2,1)S(1)} %copy-done.1, bf16[2048,512]{1,0:T(8,128)(2,1)} %wk_ref.1, bf16[2048,512]{1,0:T(8,128)(2,1)} %wv_ref.1, ...), custom_call_target="tpu_custom_call" | custom-call | flops 4831838208 | bytes 11796480 | tf_op jit(solution)/shard_map/project_qkv/pallas_call | solution.py:128
  50.7 0.0 copy-start.3
  50.7 0.8 dynamic-slice_bitcast_fusion.2
  51.5 1.0 dynamic-slice_bitcast_fusion
  52.5 1.5 collective-permute-start
  54.0 0.6 collective-permute-start.1
  54.5 0.7 fusion
  55.2 0.0 copy-start.9
  55.2 1.8 fusion.2
  57.0 0.0 copy-done.9
  57.0 1.8 multiply_multiply_fusion
  58.9 0.0 copy-start.7
  58.9 3.4 %collective-permute-start.4 = (f32[2,512]{1,0:T(2,128)S(1)}, f32[2,512]{1,0:T(2,128)S(1)}, u32[]{:S(2)}, u32[]{:S(2)}) collective-permute-start(f32[2,512]{1,0:T(2,128)S(1)} %slice.48), channel_id=1, source_target_pairs={{0,4},{4,8},{8,12},{12,16},{16,20},{20,24},{24,28},{1,5},{5,9},{9,... | collective-permute-start | bytes 12296 | tf_op jit(solution)/shard_map/ppermute | solution.py:26
  62.3 2.2 collective-permute-done.q_recv
  64.5 16.1 %collective-permute-done.1.kv_recv = bf16[768,512]{1,0:T(8,128)(2,1)S(1)} collective-permute-done((bf16[768,512]{1,0:T(8,128)(2,1)S(1)}, bf16[768,512]{1,0:T(8,128)(2,1)S(1)}, u32[]{:S(2)}, u32[]{:S(2)}) %collective-permute-start.1) | collective-permute-done | bytes 786464 | tf_op jit(solution)/shard_map/ppermute | solution.py:20
  80.6 0.9 copy-done.10
  81.5 119.9 %attend_line.1 = (bf16[2,768,256]{2,1,0:T(8,128)(2,1)}, f32[2,768,128]{2,1,0:T(8,128)}) custom-call(bf16[768,256]{1,0:T(8,128)(2,1)} %get-tuple-element.15.q_keep, bf16[768,256]{1,0:T(8,128)(2,1)} %copy-done.11, bf16[768,512]{1,0:T(8,128)(2,1)} %get-tuple-element.13.kv_keep, bf16[768,512]{1,0:T(8,128)(2,1)} %copy-done.10, f32[2]{0:T(128)} %lambdas_ref.1, ...), custom_call_target="tpu_custom_call" | custom-call | flops 7247757312 | bytes 1572864 | tf_op jit(solution)/shard_map/attend_line/pallas_call | solution.py:379
  201.4 1.0 slice_bitcast_fusion.1
  202.4 1.9 bitcast_select_fusion.3
  204.3 6.5 %collective-permute-start.2 = (bf16[768,256]{1,0:T(8,128)(2,1)}, bf16[768,256]{1,0:T(8,128)(2,1)}, u32[]{:S(2)}, u32[]{:S(2)}) collective-permute-start(bf16[768,256]{1,0:T(8,128)(2,1)} %bitcast_select_fusion.3), channel_id=1, source_target_pairs={{4,0},{0,28},{12,8},{8,20},{20,16},{16,12},{28,24},{24,4},{5,1},{1... | collective-permute-start | bytes 1179656 | tf_op jit(solution)/shard_map/ppermute | solution.py:436
  210.8 1.4 collective-permute-start.3
  212.2 0.0 collective-permute-done.4
  212.3 10.4 %fusion.20 = f32[768,2048]{1,0:T(8,128)} fusion(bf16[512,2048]{1,0:T(8,128)(2,1)S(1)} %copy-done, f32[2,512]{1,0:T(2,128)S(1)} %collective-permute-done.4, f32[768,512]{1,0:T(8,128)} %copy-done.7, bf16[2048,512]{1,0:T(8,128)(2,1)} %param.18, bf16[768,2048]{1,0:T(8,128)(2,1)} %all-gather.2.cloned.1.call-done.tok_ref, f32[2048]{0:T(1024)S(1)} %copy-done.2, ...), kind=kOutput, calls=%fused_computation.19 | convolution fusion | flops 3229876224 | bytes 15225856 | tf_op jit(solution)/shard_map/dot_general | solution.py:580
  222.7 0.0 collective-permute-done.2
  222.7 0.0 collective-permute-done.3
  222.7 1.1 bitcast_select_fusion.2
  223.8 7.0 %add_convert_fusion = bf16[768,2048]{1,0:T(8,128)(2,1)} fusion(f32[768,2048]{1,0:T(8,128)} %fusion.20, bf16[512,2048]{1,0:T(8,128)(2,1)} %param.24, bf16[768,256]{1,0:T(8,128)(2,1)S(1)} %get-tuple-element.19, bf16[768,256]{1,0:T(8,128)(2,1)S(1)} %get-tuple-element.18), kind=kOutput, calls=%fused_computation.4 | convolution fusion | flops 1615331328 | bytes 12320768 | tf_op jit(solution)/shard_map/dot_general | solution.py:579
  230.8 0.0 reduce-scatter.2.cloned.1.call-update
  230.8 1.1 copy-done.4
  232.0 0.7 collective-permute-start.6
  232.7 6.5 %collective-permute-start.5 = (f32[768,2]{1,0:T(8,128)S(1)}, f32[768,2]{1,0:T(8,128)S(1)}, u32[]{:S(2)}, u32[]{:S(2)}) collective-permute-start(f32[768,2]{1,0:T(8,128)S(1)} %bitcast_select_fusion.1), channel_id=1, source_target_pairs={{4,0},{0,28},{12,8},{8,20},{20,16},{16,12},{28,24},{24,4},{5,1},{1... | collective-permute-start | bytes 18440 | tf_op jit(solution)/shard_map/ppermute | solution.py:438
  239.2 0.0 collective-permute-done.6
  239.2 6.5 %collective-permute-done.5 = f32[768,2]{1,0:T(8,128)S(1)} collective-permute-done((f32[768,2]{1,0:T(8,128)S(1)}, f32[768,2]{1,0:T(8,128)S(1)}, u32[]{:S(2)}, u32[]{:S(2)}) %collective-permute-start.5) | collective-permute-done | bytes 6176 | tf_op jit(solution)/shard_map/ppermute | solution.py:438
  245.7 0.8 bitcast_select_fusion
  246.5 1.2 copy.16
  247.7 0.2 copy.17
  247.9 0.6 pad_maximum_fusion.3
  248.5 18.3 %reduce-scatter.2.cloned.1.call-done = bf16[192,2048]{1,0:T(8,128)(2,1)} async-done(((bf16[768,2048]{1,0:T(8,128)(2,1)}), bf16[192,2048]{1,0:T(8,128)(2,1)}) %reduce-scatter.2.cloned.1.call-update) | async-done | bytes 786448 | tf_op jit(solution)/shard_map/reduce_scatter | solution.py:577
  (21 shorter events, 0.1 us)
Async XLA Ops:
  7.2 205.1 %copy-start = (bf16[512,2048]{1,0:T(8,128)(2,1)S(1)}, bf16[512,2048]{1,0:T(8,128)(2,1)}, u32[]{:S(2)}) copy-start(bf16[512,2048]{1,0:T(8,128)(2,1)} %param.25) | copy-start | bytes 6291460
  7.2 2.6 copy-start.6
  7.2 33.6 %copy-start.2 = (f32[2048]{0:T(1024)S(1)}, f32[2048]{0:T(1024)}, u32[]{:S(2)}) copy-start(f32[2048]{0:T(1024)} %param.14) | copy-start | bytes 24580
  7.2 33.6 %all-gather.2.cloned.1.call-start = ((), (), s32[]{:S(2)}) async-start(), calls=%async_computation.1 | async-start | bytes 3932160 | tf_op jit(solution)/shard_map/all_gather | solution.py:544
  7.9 258.9 %reduce-scatter.2.cloned.1.call-start = ((), (), s32[]{:S(2)}) async-start(), calls=%async_computation.2 | async-start | bytes 3932160 | tf_op jit(solution)/shard_map/reduce_scatter | solution.py:577
  40.8 1.6 copy-start.1
  50.7 3.9 %copy-start.3 = (bf16[768,2048]{1,0:T(8,128)(2,1)S(1)}, bf16[768,2048]{1,0:T(8,128)(2,1)}, u32[]{:S(2)}) copy-start(bf16[768,2048]{1,0:T(8,128)(2,1)} %all-gather.2.cloned.1.call-done.tok_ref) | copy-start | bytes 9437188
  52.5 2.7 copy-start.8
  52.5 12.0 %collective-permute-start = (bf16[768,256]{1,0:T(8,128)(2,1)S(1)}, bf16[768,256]{1,0:T(8,128)(2,1)S(1)}, u32[]{:S(2)}, u32[]{:S(2)}) collective-permute-start(bf16[768,256]{1,0:T(8,128)(2,1)S(1)} %get-tuple-element.14), channel_id=1, source_target_pairs={{0,4},{4,0},{8,12},{12,8},{16,20},{20,16},{24,28},{28,24},{1,5},{5... | collective-permute-start | bytes 1179656 | tf_op jit(solution)/shard_map/ppermute | solution.py:20
  54.0 26.6 %collective-permute-start.1 = (bf16[768,512]{1,0:T(8,128)(2,1)S(1)}, bf16[768,512]{1,0:T(8,128)(2,1)S(1)}, u32[]{:S(2)}, u32[]{:S(2)}) collective-permute-start(bf16[768,512]{1,0:T(8,128)(2,1)S(1)} %get-tuple-element.12), channel_id=1, source_target_pairs={{0,4},{4,0},{8,12},{12,8},{16,20},{20,16},{24,28},{28,24},{1,5},{5... | collective-permute-start | bytes 2359304 | tf_op jit(solution)/shard_map/ppermute | solution.py:20
  55.2 1.8 copy-start.9
  58.9 21.7 %copy-start.7 = (f32[768,512]{1,0:T(8,128)}, f32[768,512]{1,0:T(8,128)S(1)}, u32[]{:S(2)}) copy-start(f32[768,512]{1,0:T(8,128)S(1)} %multiply_multiply_fusion) | copy-start | bytes 4718596
  58.9 153.4 %collective-permute-start.4 = (f32[2,512]{1,0:T(2,128)S(1)}, f32[2,512]{1,0:T(2,128)S(1)}, u32[]{:S(2)}, u32[]{:S(2)}) collective-permute-start(f32[2,512]{1,0:T(2,128)S(1)} %slice.48), channel_id=1, source_target_pairs={{0,4},{4,8},{8,12},{12,16},{16,20},{20,24},{24,28},{1,5},{5,9},{9,... | collective-permute-start | bytes 12296 | tf_op jit(solution)/shard_map/ppermute | solution.py:26
  64.5 16.1 %copy-start.11 = (bf16[768,256]{1,0:T(8,128)(2,1)}, bf16[768,256]{1,0:T(8,128)(2,1)S(1)}, u32[]{:S(2)}) copy-start(bf16[768,256]{1,0:T(8,128)(2,1)S(1)} %collective-permute-done.q_recv) | copy-start | bytes 1179652
  80.6 0.9 copy-start.10
  204.3 18.4 %collective-permute-start.2 = (bf16[768,256]{1,0:T(8,128)(2,1)}, bf16[768,256]{1,0:T(8,128)(2,1)}, u32[]{:S(2)}, u32[]{:S(2)}) collective-permute-start(bf16[768,256]{1,0:T(8,128)(2,1)} %bitcast_select_fusion.3), channel_id=1, source_target_pairs={{4,0},{0,28},{12,8},{8,20},{20,16},{16,12},{28,24},{24,4},{5,1},{1... | collective-permute-start | bytes 1179656 | tf_op jit(solution)/shard_map/ppermute | solution.py:436
  210.8 11.9 %collective-permute-start.3 = (bf16[768,256]{1,0:T(8,128)(2,1)S(1)}, bf16[768,256]{1,0:T(8,128)(2,1)}, u32[]{:S(2)}, u32[]{:S(2)}) collective-permute-start(bf16[768,256]{1,0:T(8,128)(2,1)S(1)} %slice_bitcast_fusion.1), channel_id=1, source_target_pairs={{4,28},{12,20},{20,12},{28,4},{5,29},{13,21},{21,13},{29,5},{6,30}... | collective-permute-start | bytes 1179656 | tf_op jit(solution)/shard_map/ppermute | solution.py:437
  212.3 10.4 %copy-start.5 = (bf16[2,768,256]{2,1,0:T(8,128)(2,1)S(1)}, bf16[2,768,256]{2,1,0:T(8,128)(2,1)}, u32[]{:S(2)}) copy-start(bf16[2,768,256]{2,1,0:T(8,128)(2,1)} %get-tuple-element.8) | copy-start | bytes 2359300
  230.8 1.1 copy-start.4
  232.0 7.2 %collective-permute-start.6 = (f32[768,2]{1,0:T(8,128)S(1)}, f32[768,2]{1,0:T(8,128)S(1)}, u32[]{:S(2)}, u32[]{:S(2)}) collective-permute-start(f32[768,2]{1,0:T(8,128)S(1)} %slice_bitcast_fusion), channel_id=1, source_target_pairs={{4,28},{12,20},{20,12},{28,4},{5,29},{13,21},{21,13},{29,5},{6,30}... | collective-permute-start | bytes 18440 | tf_op jit(solution)/shard_map/ppermute | solution.py:439
  232.7 13.0 %collective-permute-start.5 = (f32[768,2]{1,0:T(8,128)S(1)}, f32[768,2]{1,0:T(8,128)S(1)}, u32[]{:S(2)}, u32[]{:S(2)}) collective-permute-start(f32[768,2]{1,0:T(8,128)S(1)} %bitcast_select_fusion.1), channel_id=1, source_target_pairs={{4,0},{0,28},{12,8},{8,20},{20,16},{16,12},{28,24},{24,4},{5,1},{1... | collective-permute-start | bytes 18440 | tf_op jit(solution)/shard_map/ppermute | solution.py:438
Sparse Core Ops, SparseCore 0:
  9.6 31.2 all-gather.1
  230.9 35.8 reduce-scatter.1

commit v2 on v1

--- a/solution.py
+++ b/solution.py
@@ -158,54 +158,70 @@
 def attend_kernel(
     groups,
     block,
-    q_keep,
-    q_recv,
-    kv_keep,
-    kv_recv,
+    q_pair,
+    kv_pair,
     lambdas_ref,
     gain_ref,
     out_ref,
     lse_ref,
     kv_all,
     q_own,
-    q_far,
     acc,
     top,
     total,
     local_sem,
     send_right,
-    send_left,
     recv_sem,
-    far_send,
-    far_recv,
+    swap_send,
+    swap_recv,
 ):
     sp = lax.axis_index("sp")
     tp = lax.axis_index("tp")
     g, y = sp // 2, sp % 2
-    mirror = groups - 1 - g
-    rows, pair = q_keep.shape
+    _, rows, pair = q_pair.shape
     width = pair // 2
     blocks = rows // block
 
-    def at(group):
-        return (2 * group + y, tp)
+    def at(group, place):
+        return (2 * group + place, tp)
 
     loads = (
-        pltpu.make_async_copy(q_keep, q_own.at[y], local_sem.at[0]),
-        pltpu.make_async_copy(q_recv, q_own.at[1 - y], local_sem.at[1]),
-        pltpu.make_async_copy(kv_keep, kv_all.at[sp], local_sem.at[2]),
-        pltpu.make_async_copy(kv_recv, kv_all.at[2 * g + 1 - y], local_sem.at[3]),
+        pltpu.make_async_copy(kv_pair.at[y], kv_all.at[sp], local_sem.at[0]),
+        pltpu.make_async_copy(q_pair.at[y], q_own.at[y], local_sem.at[1]),
     )
     for load in loads:
         load.start()
     barrier = pltpu.get_barrier_semaphore()
-    for step in range(1, groups):
-        pl.semaphore_signal(
-            barrier, inc=1, device_id=at(lax.rem(g + step, groups)), device_id_type=MESH
-        )
-    pl.semaphore_wait(barrier, groups - 1)
-    for load in loads:
-        load.wait()
+    pl.semaphore_signal(barrier, inc=1, device_id=at(g, 1 - y), device_id_type=MESH)
+
+    @pl.when(g > 0)
+    def _():
+        pl.semaphore_signal(barrier, inc=1, device_id=at(g - 1, y), device_id_type=MESH)
+
+    @pl.when(g < groups - 1)
+    def _():
+        pl.semaphore_signal(barrier, inc=1, device_id=at(g + 1, y), device_id_type=MESH)
+
+    beside = jnp.where(g > 0, 1, 0) + jnp.where(g < groups - 1, 1, 0)
+    pl.semaphore_wait(barrier, 1 + beside)
+
+    def swap(source, target, index):
+        return pltpu.make_async_remote_copy(
+            src_ref=source,
+            dst_ref=target,
+            send_sem=swap_send.at[index],
+            recv_sem=swap_recv.at[index],
+            device_id=at(g, 1 - y),
+            device_id_type=MESH,
+        )
+
+    swaps = (
+        swap(kv_pair.at[1 - y], kv_all.at[sp], 0),
+        swap(q_pair.at[1 - y], q_own.at[y], 1),
+    )
+    for one_swap in swaps:
+        one_swap.start()
+    loads[0].wait()
 
     def right(chunk):
         return pltpu.make_async_remote_copy(
@@ -213,39 +229,13 @@
             dst_ref=kv_all.at[chunk],
             send_sem=send_right.at[chunk],
             recv_sem=recv_sem.at[chunk],
-            device_id=at(jnp.minimum(g + 1, groups - 1)),
+            device_id=at(jnp.minimum(g + 1, groups - 1), y),
             device_id_type=MESH,
         )
-
-    def left(chunk):
-        return pltpu.make_async_remote_copy(
-            src_ref=kv_all.at[chunk],
-            dst_ref=kv_all.at[chunk],
-            send_sem=send_left.at[chunk],
-            recv_sem=recv_sem.at[chunk],
-            device_id=at(jnp.maximum(g - 1, 0)),
-            device_id_type=MESH,
-        )
-
-    far = pltpu.make_async_remote_copy(
-        src_ref=q_own.at[1],
-        dst_ref=q_far,
-        send_sem=far_send,
-        recv_sem=far_recv,
-        device_id=at(mirror),
-        device_id_type=MESH,
-    )
-    far.start()
 
     @pl.when(g < groups - 1)
     def _():
-        right(2 * g + 1).start()
-        right(2 * g).start()
-
-    @pl.when(g > 0)
-    def _():
-        left(2 * g).start()
-        left(2 * g + 1).start()
+        right(sp).start()
 
     acc[...] = jnp.zeros_like(acc)
     total[...] = jnp.zeros_like(total)
@@ -265,16 +255,14 @@
 
     def scores_of(r, j, start, chunk, length):
         cols = slice(j * width, (j + 1) * width)
-        queries = q_use[r, pl.ds(start, block), cols]
+        queries = q_own[r, pl.ds(start, block), cols]
         keys = kv_all[chunk, :length, cols]
         return lax.dot_general(
             queries, keys, (((1,), (1,)), ((), ())), preferred_element_type=jnp.float32
         )
 
-    q_use = q_own
-
     def process(r, chunk):
-        q_chunk = jnp.where(r == 0, 2 * g, 2 * mirror + 1)
+        q_chunk = 2 * g + r
 
         @pl.when(chunk < q_chunk)
         def _():
@@ -297,45 +285,36 @@
                     scores = jnp.where(key_at <= query_at, scores, MASKED)
                     update(r, j, b * block, scores, kv_all[chunk, :length, pair:])
 
-    far.wait()
-    swap = pltpu.make_async_copy(q_far, q_own.at[1], local_sem.at[0])
-    swap.start()
-    swap.wait()
+    loads[1].wait()
+    swaps[0].wait()
+
+    @pl.when(g < groups - 1)
+    def _():
+        right(2 * g + 1 - y).start()
+
+    swaps[1].wait()
 
     def visit(i, carry):
-        step, half, side = i // 4, (i // 2) % 2, i % 2
-        group = jnp.where(side == 0, g - step, g + step)
-        chunk = jnp.where(side == 0, 2 * group + 1 - half, 2 * group + half)
-        exists = jnp.logical_and(group >= 0, group < groups)
-        exists = jnp.logical_and(exists, jnp.logical_or(step > 0, side == 0))
-
-        @pl.when(exists)
+        step, half = i // 2, i % 2
+        group = g - step
+        chunk = 2 * group + jnp.where(half == 0, y, 1 - y)
+
+        @pl.when(step > 0)
         def _():
-            @pl.when(jnp.logical_and(step > 0, side == 0))
+            right(chunk).wait_recv()
+
+            @pl.when(g < groups - 1)
             def _():
-                right(chunk).wait_recv()
-
-                @pl.when(g < groups - 1)
-                def _():
-                    right(chunk).start()
-
-            @pl.when(jnp.logical_and(step > 0, side == 1))
-            def _():
-                left(chunk).wait_recv()
-
-                @pl.when(g > 0)
-                def _():
-                    left(chunk).start()
-
-            def each(r, inner):
-                process(r, chunk)
-                return inner
-
-            lax.fori_loop(0, 2, each, 0)
-
+                right(chunk).start()
+
+        def each(r, inner):
+            process(r, chunk)
+            return inner
+
+        lax.fori_loop(0, 2, each, 0)
         return carry
 
-    lax.fori_loop(0, 4 * groups, visit, 0)
+    lax.fori_loop(0, 2 * g + 2, visit, 0)
 
     lam = lambdas_ref[y]
     gain = gain_ref[...] * HEAD_KEEP
@@ -356,21 +335,16 @@
     lax.fori_loop(0, 2 * blocks, close, 0)
 
     def drain(chunk, carry):
-        @pl.when(jnp.logical_and(g < groups - 1, chunk < 2 * g + 2))
-        def _():
-            right(chunk).wait_send()
-
-        @pl.when(jnp.logical_and(g > 0, chunk >= 2 * g))
-        def _():
-            left(chunk).wait_send()
-
+        right(chunk).wait_send()
         return carry
 
-    lax.fori_loop(0, 2 * groups, drain, 0)
-
-
-def attend(groups, q_keep, q_recv, kv_keep, kv_recv, lambdas, head_gain):
-    rows, pair = q_keep.shape
+    @pl.when(g < groups - 1)
+    def _():
+        lax.fori_loop(0, 2 * g + 2, drain, 0)
+
+
+def attend(groups, q_pair, kv_pair, lambdas, head_gain):
+    _, rows, pair = q_pair.shape
     block = rows // 3 if rows % 48 == 0 else rows
     vmem = pl.BlockSpec(memory_space=pltpu.VMEM)
     anywhere = pl.BlockSpec(memory_space=pl.ANY)
@@ -382,21 +356,19 @@
             jax.ShapeDtypeStruct((2, rows, pair), jnp.bfloat16),
             jax.ShapeDtypeStruct((2, rows, lanes), jnp.float32),
         ),
-        in_specs=[anywhere] * 4 + [pl.BlockSpec(memory_space=pltpu.SMEM), vmem],
+        in_specs=[anywhere] * 2 + [pl.BlockSpec(memory_space=pltpu.SMEM), vmem],
         out_specs=(vmem, vmem),
         scratch_shapes=[
             pltpu.VMEM((chunks, rows, 2 * pair), jnp.bfloat16),
             pltpu.VMEM((2, rows, pair), jnp.bfloat16),
-            pltpu.VMEM((rows, pair), jnp.bfloat16),
             pltpu.VMEM((2, 2, rows, pair), jnp.float32),
             pltpu.VMEM((2, 2, rows, lanes), jnp.float32),
             pltpu.VMEM((2, 2, rows, lanes), jnp.float32),
-            pltpu.SemaphoreType.DMA((4,)),
+            pltpu.SemaphoreType.DMA((2,)),
             pltpu.SemaphoreType.DMA((chunks,)),
             pltpu.SemaphoreType.DMA((chunks,)),
-            pltpu.SemaphoreType.DMA((chunks,)),
-            pltpu.SemaphoreType.DMA,
-            pltpu.SemaphoreType.DMA,
+            pltpu.SemaphoreType.DMA((2,)),
+            pltpu.SemaphoreType.DMA((2,)),
         ],
         compiler_params=pltpu.CompilerParams(
             collective_id=0, has_side_effects=True, vmem_limit_bytes=56 * 2**20
@@ -407,7 +379,7 @@
             transcendentals=0,
         ),
         name="attend_line",
-    )(q_keep, q_recv, kv_keep, kv_recv, lambdas, head_gain[None, :])
+    )(q_pair, kv_pair, lambdas, head_gain[None, :])
 
 
 def attention_by_head(tokens, norm_gain, w_query, w_key, w_value, lambdas, head_gain, positions):
@@ -419,28 +391,15 @@
     queries, key_values = project(
         tokens, norm_gain, w_query, w_key, w_value, positions, head_count, head_width
     )
-    take = lambda array, index: lax.dynamic_index_in_dim(array, index, 0, keepdims=False)
-    kv_recv = partner(take(key_values, 1 - y), "sp", 0)
-    q_recv = partner(take(queries, 1 - y), "sp", 0)
-    result, lse = attend(
-        groups, take(queries, y), q_recv, take(key_values, y), kv_recv, lambdas, head_gain
-    )
+    result, lse = attend(groups, queries, key_values, lambdas, head_gain)
     lse = lse[:, :, :2]
-    cross = []
-    second = []
-    for group in range(groups):
-        far = 2 * (groups - 1 - group) + 1
-        cross += [(2 * group + 1, 2 * group), (2 * group, far)]
-        second += [(2 * group + 1, far)]
-    mine = jnp.where(y == 1, result[0], result[1])
-    crossed = lax.ppermute(mine, "sp", cross)
-    seconded = lax.ppermute(result[1], "sp", second)
-    crossed_lse = lax.ppermute(jnp.where(y == 1, lse[0], lse[1]), "sp", cross)
-    seconded_lse = lax.ppermute(lse[1], "sp", second)
-    first = jnp.where(y == 0, result[0], crossed)
-    last = jnp.where(y == 0, crossed, seconded)
-    first_lse = jnp.where(y == 0, lse[0], crossed_lse)
-    last_lse = jnp.where(y == 0, crossed_lse, seconded_lse)
+    at_first = y == 0
+    crossed = partner(jnp.where(at_first, result[1], result[0]), "sp", 0)
+    crossed_lse = partner(jnp.where(at_first, lse[1], lse[0]), "sp", 0)
+    first = jnp.where(at_first, result[0], crossed)
+    last = jnp.where(at_first, crossed, result[1])
+    first_lse = jnp.where(at_first, lse[0], crossed_lse)
+    last_lse = jnp.where(at_first, crossed_lse, lse[1])
     return (
         jnp.concatenate([first, last], axis=1),
         jnp.concatenate([first_lse, last_lse], axis=1),
@@ -552,7 +511,7 @@
     def product_of(weight):
         return inv_rms * jnp.dot(scaled, weight, preferred_element_type=jnp.float32)
 
-    if head_count == 2 and head_width == 128 and count % 4 == 0:
+    if head_count == 2 and head_width == 128 and count % 2 == 0:
         attended, row_lse = attention_by_head(
             gathered, norm_gain, w_query, w_key, w_value, lambdas, head_gain, positions
         )

time: 274 us -> 243 us (0.89)
  Pallas kernels: 128 us -> 49.9 us
  waiting for transfers between devices: 74.9 us -> 138 us
  starting transfers between devices: 20.6 us -> 5.55 us
  local copies, waits for them, and re-layouts: 7.87 us -> 4.59 us
    reduce_scatter x1, waiting for transfers between devices: 18.3 us -> 97.8 us  [per_device(): lax.psum_scatter((jnp.dot(attended, attend_proj, preferred_element_type=j...]
    pallas_call x1, Pallas kernels: 120 us -> 41.4 us  [attend(): pl.pallas_call(functools.partial(attend_kernel, groups, block), out_shape...]
    ppermute x4 -> x0, starting transfers between devices: 15.1 us -> none  [the longest x1 6.54 us: attention_by_head(): crossed_lse = lax.ppermute(jnp.where(y == 1, lse[0], lse[1]), 'sp', cross)]
    ppermute x2, waiting for transfers between devices: 18.3 us -> 8.31 us  [partner(): lax.ppermute(value, axis, [(i, i ^ 1 << stride) for i in range(lax.axis_s...]
    ppermute x4 -> x0, waiting for transfers between devices: 6.48 us -> none  [the longest x1 6.47 us: attention_by_head(): crossed_lse = lax.ppermute(jnp.where(y == 1, lse[0], lse[1]), 'sp', cross)]
    squeeze x4 -> x0, local copies, waits for them, and re-layouts: 2.86 us -> none  [the longest x2 1.81 us: attention_by_head(): lax.dynamic_index_in_dim(array, index, 0, keepdims=False)]
  transfers between devices with their start and end apart: 9 -> 5, of which waited for: 5 -> 3; matrix products, arithmetic and copies ran while one was open for 8% -> 7% of each run, Pallas kernels for 44% -> 21%
where the time goes in v2:
time: 243 us
  waiting for transfers between devices  138 us (57%)
  Pallas kernels  49.9 us (21%)
  matrix products  22.7 us (9%)
  between operations  14.2 us (6%)
  other arithmetic  7.91 us (3%)
  starting transfers between devices  5.55 us (2%)
  local copies, waits for them, and re-layouts  4.59 us (2%)
    reduce_scatter x1, waiting for transfers between devices, per_device(): lax.psum_scatter((jnp.dot(attended, attend_proj, preferred_element_type=j...  97.8 us
    pallas_call x1, Pallas kernels, attend(): pl.pallas_call(functools.partial(attend_kernel, groups, block), out_shape...  41.4 us
    all_gather x1, waiting for transfers between devices, per_device(): gathered = lax.all_gather(tokens, 'tp', axis=1, tiled=True)  31 us
    dot_general x1, matrix products, per_device(): jnp.dot(convolved, convolve_proj, preferred_element_type=jnp.float32)  10.4 us
    pallas_call x1, Pallas kernels, project(): pl.pallas_call(functools.partial(project_kernel, head_width ** (-0.5) * L...  8.45 us
    ppermute x2, waiting for transfers between devices, partner(): lax.ppermute(value, axis, [(i, i ^ 1 << stride) for i in range(lax.axis_s...  8.31 us
    dot_general x1, matrix products, per_device(): jnp.dot(attended, attend_proj, preferred_element_type=jnp.float32)  6.98 us
    dot_general x2, matrix products, product_of(): return inv_rms * jnp.dot(scaled, weight, preferred_element_type=jnp.float32)  5.34 us
  transfers between devices with their start and end apart: 5, of which 3 were waited for; matrix products, arithmetic and copies ran while one was open for 7% of the time, Pallas kernels for 21%

profile of v2, /device:TPU:0, one launch (start us, length us, event | category | flops | bytes accessed | tf_op | source)
XLA Modules:
  0.0 242.7 jit_solution(8771024620407991104)
XLA Ops:
  7.2 0.0 copy-start
  7.2 0.0 copy-start.8
  7.2 0.0 all-gather.2.cloned.1.call-start
  7.2 0.7 all-gather.2.cloned.1.call-update
  7.9 0.0 reduce-scatter.2.cloned.1.call-start
  8.0 1.4 fusion.29
  9.5 0.0 copy-start.2
  9.5 0.3 pad_maximum_fusion.1
  9.8 0.0 copy-done.8
  9.8 31.0 %all-gather.2.cloned.1.call-done.tok_ref = bf16[768,2048]{1,0:T(8,128)(2,1)} async-done(((bf16[768,512]{1,0:T(8,128)(2,1)}), bf16[768,2048]{1,0:T(8,128)(2,1)}) %all-gather.2.cloned.1.call-update) | async-done | bytes 3145744 | tf_op jit(solution)/shard_map/all_gather | solution.py:503
  40.8 0.0 copy-start.5
  40.8 2.7 %fusion = f32[768]{0:T(1024)S(1)} fusion(bf16[768,2048]{1,0:T(8,128)(2,1)} %all-gather.2.cloned.1.call-done.tok_ref), kind=kLoop, calls=%fused_computation.2 | loop fusion | flops 4717824 | bytes 3148800 | tf_op jit(solution)/shard_map/reduce_sum | solution.py:506
  43.6 0.0 copy-done.2
  43.6 0.1 copy-done.5
  43.7 0.0 copy-start.10
  43.7 3.5 %fusion.2 = f32[768,512]{1,0:T(8,128)S(1)} fusion(bf16[2048,512]{1,0:T(8,128)(2,1)} %param.20, bf16[768,2048]{1,0:T(8,128)(2,1)S(1)} %copy-done.5, f32[2048]{0:T(1024)S(1)} %copy-done.2), kind=kOutput, calls=%fused_computation.5 | convolution fusion | flops 1615331328 | bytes 6823936 | tf_op jit(solution)/shard_map/dot_general | solution.py:512
  47.2 0.0 copy-done.10
  47.2 0.0 copy-start.1
  47.2 1.8 multiply_multiply_fusion
  49.0 0.0 copy-start.9
  49.1 3.4 %collective-permute-start.1 = (f32[2,512]{1,0:T(2,128)S(1)}, f32[2,512]{1,0:T(2,128)S(1)}, u32[]{:S(2)}, u32[]{:S(2)}) collective-permute-start(f32[2,512]{1,0:T(2,128)S(1)} %slice.48), channel_id=1, source_target_pairs={{0,4},{4,8},{8,12},{12,16},{16,20},{20,24},{24,28},{1,5},{5,9},{9,... | collective-permute-start | bytes 12296 | tf_op jit(solution)/shard_map/ppermute | solution.py:26
  52.4 0.0 copy-done.9
  52.4 0.0 copy-done.1
  52.5 8.5 %project_qkv.1 = (bf16[2,768,256]{2,1,0:T(8,128)(2,1)S(1)}, bf16[2,768,512]{2,1,0:T(8,128)(2,1)S(1)}) custom-call(bf16[768,2048]{1,0:T(8,128)(2,1)} %all-gather.2.cloned.1.call-done.tok_ref, f32[1,2048]{1,0:T(1,128)S(1)} %bitcast.22, bf16[2048,512]{1,0:T(8,128)(2,1)S(1)} %copy-done.1, bf16[2048,512]{1,0:T(8,128)(2,1)} %wk_ref.1, bf16[2048,512]{1,0:T(8,128)(2,1)} %wv_ref.1, ...), custom_call_target="tpu_custom_call" | custom-call | flops 4831838208 | bytes 11796480 | tf_op jit(solution)/shard_map/project_qkv/pallas_call | solution.py:128
  60.9 0.0 copy-start.3
  60.9 1.2 copy-done.3
  62.1 0.0 copy-start.4
  62.1 0.9 copy-done.4
  63.0 41.4 %attend_line.1 = (bf16[2,768,256]{2,1,0:T(8,128)(2,1)}, f32[2,768,128]{2,1,0:T(8,128)}) custom-call(bf16[2,768,256]{2,1,0:T(8,128)(2,1)} %copy-done.4, bf16[2,768,512]{2,1,0:T(8,128)(2,1)} %copy-done.3, f32[2]{0:T(128)} %lambdas_ref.1, f32[1,256]{1,0:T(1,128)} %bitcast.26), custom_call_target="tpu_custom_call" | custom-call | flops 7247757312 | bytes 1572864 | tf_op jit(solution)/shard_map/attend_line/pallas_call | solution.py:353
  104.4 1.9 bitcast_select_fusion.4
  106.3 0.5 collective-permute-start
  106.8 0.0 collective-permute-done.1
  106.8 0.0 copy-done
  106.8 0.0 copy-start.7
  106.8 10.4 %fusion.20 = f32[768,2048]{1,0:T(8,128)} fusion(bf16[512,2048]{1,0:T(8,128)(2,1)S(1)} %copy-done, f32[2,512]{1,0:T(2,128)S(1)} %collective-permute-done.1, f32[768,512]{1,0:T(8,128)} %copy-done.9, bf16[2048,512]{1,0:T(8,128)(2,1)} %param.18, bf16[768,2048]{1,0:T(8,128)(2,1)} %all-gather.2.cloned.1.call-done.tok_ref, f32[2048]{0:T(1024)S(1)} %copy-done.2, ...), kind=kOutput, calls=%fused_computation.19 | convolution fusion | flops 3229876224 | bytes 15225856 | tf_op jit(solution)/shard_map/dot_general | solution.py:539
  117.2 0.0 collective-permute-done
  117.2 0.0 copy-done.7
  117.2 0.1 bitcast_select_fusion.5
  117.3 7.0 %add_convert_fusion = bf16[768,2048]{1,0:T(8,128)(2,1)} fusion(f32[768,2048]{1,0:T(8,128)} %fusion.20, bf16[512,2048]{1,0:T(8,128)(2,1)} %param.24, bf16[768,256]{1,0:T(8,128)(2,1)S(1)} %get-tuple-element.15, bf16[768,256]{1,0:T(8,128)(2,1)S(1)} %get-tuple-element.14), kind=kOutput, calls=%fused_computation.4 | convolution fusion | flops 1615331328 | bytes 12320768 | tf_op jit(solution)/shard_map/dot_general | solution.py:538
  124.3 0.0 reduce-scatter.2.cloned.1.call-update
  124.3 1.1 copy-done.6
  125.4 1.6 collective-permute-start.2
  127.0 8.3 %collective-permute-done.2 = f32[768,2]{1,0:T(8,128)S(1)} collective-permute-done((f32[768,2]{1,0:T(8,128)S(1)}, f32[768,2]{1,0:T(8,128)S(1)}, u32[]{:S(2)}, u32[]{:S(2)}) %collective-permute-start.2) | collective-permute-done | bytes 6176 | tf_op jit(solution)/shard_map/ppermute | solution.py:20
  135.3 0.8 bitcast_select_fusion.2
  136.1 1.1 copy.16
  137.3 0.2 copy.17
  137.4 0.6 pad_maximum_fusion.3
  138.1 97.8 %reduce-scatter.2.cloned.1.call-done = bf16[192,2048]{1,0:T(8,128)(2,1)} async-done(((bf16[768,2048]{1,0:T(8,128)(2,1)}), bf16[192,2048]{1,0:T(8,128)(2,1)}) %reduce-scatter.2.cloned.1.call-update) | async-done | bytes 786448 | tf_op jit(solution)/shard_map/reduce_scatter | solution.py:536
  (7 shorter events, 0.1 us)
Async XLA Ops:
  7.2 99.6 %copy-start = (bf16[512,2048]{1,0:T(8,128)(2,1)S(1)}, bf16[512,2048]{1,0:T(8,128)(2,1)}, u32[]{:S(2)}) copy-start(bf16[512,2048]{1,0:T(8,128)(2,1)} %param.25) | copy-start | bytes 6291460
  7.2 2.6 %copy-start.8 = (bf16[3,512]{1,0:T(4,128)(2,1)S(1)}, bf16[3,512]{1,0:T(4,128)(2,1)}, u32[]{:S(2)}) copy-start(bf16[3,512]{1,0:T(4,128)(2,1)} %param.21) | copy-start | bytes 9220
  7.2 33.6 %all-gather.2.cloned.1.call-start = ((), (), s32[]{:S(2)}) async-start(), calls=%async_computation.1 | async-start | bytes 3932160 | tf_op jit(solution)/shard_map/all_gather | solution.py:503
  7.9 227.9 %reduce-scatter.2.cloned.1.call-start = ((), (), s32[]{:S(2)}) async-start(), calls=%async_computation.2 | async-start | bytes 3932160 | tf_op jit(solution)/shard_map/reduce_scatter | solution.py:536
  9.5 34.1 %copy-start.2 = (f32[2048]{0:T(1024)S(1)}, f32[2048]{0:T(1024)}, u32[]{:S(2)}) copy-start(f32[2048]{0:T(1024)} %param.14) | copy-start | bytes 24580
  40.8 2.8 %copy-start.5 = (bf16[768,2048]{1,0:T(8,128)(2,1)S(1)}, bf16[768,2048]{1,0:T(8,128)(2,1)}, u32[]{:S(2)}) copy-start(bf16[768,2048]{1,0:T(8,128)(2,1)} %all-gather.2.cloned.1.call-done.tok_ref) | copy-start | bytes 9437188
  43.7 3.5 %copy-start.10 = (bf16[2048,512]{1,0:T(8,128)(2,1)S(1)}, bf16[2048,512]{1,0:T(8,128)(2,1)}, u32[]{:S(2)}) copy-start(bf16[2048,512]{1,0:T(8,128)(2,1)} %param.19) | copy-start | bytes 6291460
  47.2 5.2 %copy-start.1 = (bf16[2048,512]{1,0:T(8,128)(2,1)S(1)}, bf16[2048,512]{1,0:T(8,128)(2,1)}, u32[]{:S(2)}) copy-start(bf16[2048,512]{1,0:T(8,128)(2,1)} %wq_ref.1) | copy-start | bytes 6291460
  49.0 3.4 %copy-start.9 = (f32[768,512]{1,0:T(8,128)}, f32[768,512]{1,0:T(8,128)S(1)}, u32[]{:S(2)}) copy-start(f32[768,512]{1,0:T(8,128)S(1)} %multiply_multiply_fusion) | copy-start | bytes 4718596
  49.1 57.8 %collective-permute-start.1 = (f32[2,512]{1,0:T(2,128)S(1)}, f32[2,512]{1,0:T(2,128)S(1)}, u32[]{:S(2)}, u32[]{:S(2)}) collective-permute-start(f32[2,512]{1,0:T(2,128)S(1)} %slice.48), channel_id=1, source_target_pairs={{0,4},{4,8},{8,12},{12,16},{16,20},{20,24},{24,28},{1,5},{5,9},{9,... | collective-permute-start | bytes 12296 | tf_op jit(solution)/shard_map/ppermute | solution.py:26
  60.9 1.2 copy-start.3
  62.1 0.9 copy-start.4
  106.3 10.9 %collective-permute-start = (bf16[768,256]{1,0:T(8,128)(2,1)}, bf16[768,256]{1,0:T(8,128)(2,1)S(1)}, u32[]{:S(2)}, u32[]{:S(2)}) collective-permute-start(bf16[768,256]{1,0:T(8,128)(2,1)} %bitcast_select_fusion.4), channel_id=1, source_target_pairs={{0,4},{4,0},{8,12},{12,8},{16,20},{20,16},{24,28},{28,24},{1,5},{5... | collective-permute-start | bytes 1179656 | tf_op jit(solution)/shard_map/ppermute | solution.py:20
  106.8 10.4 %copy-start.7 = (bf16[2,768,256]{2,1,0:T(8,128)(2,1)S(1)}, bf16[2,768,256]{2,1,0:T(8,128)(2,1)}, u32[]{:S(2)}) copy-start(bf16[2,768,256]{2,1,0:T(8,128)(2,1)} %get-tuple-element.8) | copy-start | bytes 2359300
  124.3 1.1 copy-start.6
  125.4 9.9 %collective-permute-start.2 = (f32[768,2]{1,0:T(8,128)S(1)}, f32[768,2]{1,0:T(8,128)S(1)}, u32[]{:S(2)}, u32[]{:S(2)}) collective-permute-start(f32[768,2]{1,0:T(8,128)S(1)} %bitcast_select_fusion.1), channel_id=1, source_target_pairs={{0,4},{4,0},{8,12},{12,8},{16,20},{20,16},{24,28},{28,24},{1,5},{5... | collective-permute-start | bytes 18440 | tf_op jit(solution)/shard_map/ppermute | solution.py:20
Sparse Core Ops, SparseCore 0:
  9.6 31.2 all-gather.1
  124.4 111.3 reduce-scatter.1
